TPU v7x, 512 devices: a whole 4x4x16 slice. The times are simulated.
512 devices in a mesh: ep: 32 (over z, core), tp: 16 (over y, x).
Axes of the slice: x: 4, y: 4, z: 16, core: 2. Of those that a mesh axis runs over, the one named last changes fastest.
Arguments:
- conv_input: bfloat16 [1024, 65536], P('tp', 'ep'), may hold values from -6 to 6
- out_gate: bfloat16 [1024, 65536], P('tp', 'ep'), may hold values from -6 to 6
- in_gate: bfloat16 [1024, 65536], P('tp', 'ep'), may hold values from -6 to 6
- conv_taps: float32 [3, 1024], replicated, may hold values from -3.5 to 3.5
- mixer_proj: bfloat16 [1024, 2048], P(None, 'tp'), may hold values from -0.1875 to 0.1875
- token_rows: bfloat16 [8192, 2048], P('ep', 'tp'), may hold values from -4000 to 4000
- routes: int32 [8192, 2], P('ep'), may hold values from 0 to 31, as said below
- route_weights: float32 [8192, 2], P('ep'), may hold values from 0.3 to 1
- expert_gate: bfloat16 [32, 2048, 4096], P('ep', None, 'tp'), may hold values from -0.125 to 0.125
- expert_up: bfloat16 [32, 2048, 4096], P('ep', None, 'tp'), may hold values from -0.125 to 0.125
- expert_down: bfloat16 [32, 4096, 2048], P('ep', 'tp'), may hold values from -0.125 to 0.125
Outputs:
- mixed_out: bfloat16 [65536, 2048], P('ep', 'tp')
- expert_out: bfloat16 [8192, 2048], P('ep', 'tp')
Inputs may be any that keep to these rules, and one draw needn't show every extreme that they name: `routes`: in each aligned block of 256 rows, no expert is named more than 32 times and one expert, the same in every block, exactly 32 times; the two experts of a row differ.
All inputs are finite; a program needn't handle non-finite values.
Results may differ from a plain program's by a relative error of at most 0.015.
Values may be sent and summed in bfloat16 or wider, within the bound.
No kernel may reach another device: no remote copies, remote signals or barrier semaphores. Data moves between devices by JAX's collectives and lax.ppermute only.
A program may use at most 64 MiB of HBM per device.

v0:
```python
import jax
import jax.numpy as jnp
from jax import lax
from jax.experimental import pallas as pl
from jax.experimental.pallas import tpu as pltpu
from jax.sharding import Mesh
from jax.sharding import PartitionSpec as P

KERNEL = 3
EPSILON = 1e-06
BF = jnp.bfloat16
F32 = jnp.float32


def expert_kernel(me_ref, x_ref, gate_ref, up_ref, down_ref, out_ref):
    parts = x_ref.shape[0]
    cols = x_ref.shape[2]
    side = 4
    core = me_ref[0] // parts
    natural = [j for j in range(parts)]
    turned = [(j % side) * side + j // side for j in range(parts)]
    load = [jnp.where(core == 0, natural[j], turned[j]) for j in range(parts)]
    store = [jnp.where(core == 0, turned[j], natural[j]) for j in range(parts)]
    x = jnp.concatenate([x_ref[load[j]] for j in range(parts)], axis=1)
    values = x.astype(F32)
    squares = jnp.sum(values * values, axis=1, keepdims=True)
    scale = lax.rsqrt(squares / (parts * cols) + EPSILON)
    gate = scale * jnp.dot(x, gate_ref[...], preferred_element_type=F32)
    up = scale * jnp.dot(x, up_ref[...], preferred_element_type=F32)
    hidden = (jax.nn.silu(gate) * up).astype(BF)
    part = jnp.dot(hidden, down_ref[...], preferred_element_type=F32).astype(BF)
    for j in range(parts):
        out_ref[store[j]] = part[:, j * cols : (j + 1) * cols]


def expert_part(me, x, gate_weight, up_weight, down_weight, tile):
    parts, rows, cols = x.shape
    whole = lambda w: pl.BlockSpec(w.shape, lambda i, c: (0, 0))
    return pl.pallas_call(
        expert_kernel,
        grid_spec=pltpu.PrefetchScalarGridSpec(
            num_scalar_prefetch=1,
            grid=(rows // tile,),
            in_specs=[
                pl.BlockSpec((parts, tile, cols), lambda i, c: (0, i, 0)),
                whole(gate_weight),
                whole(up_weight),
                whole(down_weight),
            ],
            out_specs=pl.BlockSpec((parts, tile, cols), lambda i, c: (0, i, 0)),
        ),
        out_shape=jax.ShapeDtypeStruct(x.shape, BF),
        compiler_params=pltpu.CompilerParams(vmem_limit_bytes=28 * 1024 * 1024),
        cost_estimate=pl.CostEstimate(
            flops=6 * rows * parts * cols * gate_weight.shape[1],
            bytes_accessed=2 * 2 * rows * parts * cols + 6 * gate_weight.size,
            transcendentals=rows * gate_weight.shape[1],
        ),
    )(me.reshape(1), x, gate_weight, up_weight, down_weight)


def mixer_kernel(me_ref, y0_ref, y1_ref, y2a_ref, y2b_ref, y3_ref, proj_ref, out_ref):
    blocks = proj_ref.shape[0]
    side = 4
    core = me_ref[0] // blocks
    row = (me_ref[0] % blocks) // side
    col = me_ref[0] % side
    weights = []
    for far in range(side):
        for near in range(side):
            down = jnp.where(core == 0, far, near)
            right = jnp.where(core == 0, near, far)
            at = ((row + down) % side) * side + (col + right) % side
            weights.append(proj_ref[at])
    proj = jnp.concatenate(weights, axis=0)
    pieces = [
        ref[i]
        for ref in (y0_ref, y1_ref, y2a_ref, y2b_ref, y3_ref)
        for i in range(ref.shape[0])
    ]
    y = jnp.concatenate(pieces, axis=0)
    flat = lax.dot_general(
        proj, y, (((0,), (0,)), ((), ())), preferred_element_type=F32
    )
    out_ref[...] = jnp.transpose(flat).astype(BF)


def mixer_product(me, pieces, proj, tile):
    length = pieces[0].shape[2]
    blocks, width, cols = proj.shape
    return pl.pallas_call(
        mixer_kernel,
        grid_spec=pltpu.PrefetchScalarGridSpec(
            num_scalar_prefetch=1,
            grid=(length // tile,),
            in_specs=[
                pl.BlockSpec(p.shape[:2] + (tile,), lambda i, c: (0, 0, i)) for p in pieces
            ]
            + [pl.BlockSpec(proj.shape, lambda i, c: (0, 0, 0))],
            out_specs=pl.BlockSpec((tile, cols), lambda i, c: (i, 0)),
        ),
        out_shape=jax.ShapeDtypeStruct((length, cols), BF),
        compiler_params=pltpu.CompilerParams(vmem_limit_bytes=20 * 1024 * 1024),
        cost_estimate=pl.CostEstimate(
            flops=2 * length * blocks * width * cols,
            bytes_accessed=2 * length * (blocks * width + cols) + 2 * proj.size,
            transcendentals=0,
        ),
    )(me.reshape(1), *pieces, proj)


def sum_parts(arrived):
    return arrived.astype(F32).sum(axis=0).astype(BF)


def layer(
    conv_input,
    out_gate,
    in_gate,
    conv_taps,
    mixer_proj,
    token_rows,
    routes,
    route_weights,
    expert_gate,
    expert_up,
    expert_down,
):
    depth = lax.axis_size("z")
    experts = 2 * depth
    tp = lax.axis_size("tp")
    core = lax.axis_index("c")
    me = lax.axis_index(("c", "tp"))
    rows_b, cols_part = token_rows.shape
    capacity = 4 * rows_b // experts
    slot_total = experts * capacity
    half = slot_total // 2

    expert_ids = jnp.arange(experts, dtype=jnp.int32)[None, :]
    hit0 = routes[:, 0:1] == expert_ids
    hit1 = routes[:, 1:2] == expert_ids
    hits = (hit0 | hit1).astype(BF)
    order = jnp.arange(rows_b, dtype=jnp.int32)
    earlier_rows = (order[None, :] < order[:, None]).astype(BF)
    earlier = jnp.dot(earlier_rows, hits, preferred_element_type=F32).astype(jnp.int32)
    places = []
    for k, hit in enumerate((hit0, hit1)):
        slot = jnp.sum(jnp.where(hit, earlier, 0), axis=1)
        places.append((routes[:, k] ^ core) * capacity + slot)
    slot_ids = jnp.arange(slot_total, dtype=jnp.int32)[None, :]
    pick0 = places[0][:, None] == slot_ids
    pick1 = places[1][:, None] == slot_ids
    pick_any = (pick0 | pick1).astype(BF)
    outgoing = lax.dot_general(
        pick_any, token_rows, (((0,), (0,)), ((), ())), preferred_element_type=F32
    ).astype(BF)

    outgoing, conv_input, in_gate = lax.optimization_barrier((outgoing, conv_input, in_gate))
    arrived = lax.all_to_all(
        outgoing.reshape(depth, 2, capacity, cols_part), "z", 0, 0, tiled=True
    )

    length = conv_input.shape[1]
    width_part = conv_input.shape[0]
    offset = lax.axis_index("tp") * width_part
    local_taps = lax.dynamic_slice_in_dim(conv_taps, offset, width_part, 1)
    z_rows = (conv_input.astype(F32) * in_gate.astype(F32)).astype(BF)
    pairs = [(i, i + 1) for i in range(experts - 1)]
    rim = lax.ppermute(z_rows[:, length - (KERNEL - 1) :], ("z", "c"), pairs)
    longer = jnp.concatenate([rim, z_rows], axis=1).astype(F32)
    conv_sum = jnp.zeros(z_rows.shape, F32)
    for lag in range(KERNEL):
        begin = KERNEL - 1 - lag
        conv_sum = conv_sum + local_taps[lag][:, None] * longer[:, begin : begin + length]
    gated = (out_gate.astype(F32) * conv_sum).astype(BF)
    side = 4
    swap = [(0, 1), (1, 0)]
    place = lambda c, y, x: (c * side + y) * side + x
    span = range(side)
    along_x = lambda c: [[place(c, y, x) for x in span] for y in span]
    along_y = lambda c: [[place(c, y, x) for y in span] for x in span]
    early = along_x(0) + along_y(1)
    late = along_y(0) + along_x(1)

    def step(value, by, phase):
        pairs = []
        for c in range(2):
            for y in span:
                for x in span:
                    if (c == 0) == (phase == 0):
                        to = place(c, y, (x + by) % side)
                    else:
                        to = place(c, (y + by) % side, x)
                    pairs.append((place(c, y, x), to))
        return lax.ppermute(value, ("c", "tp"), pairs)

    gated = gated.reshape(2, width_part // 2, length)
    before = step(gated, 1, 0)
    after = step(gated, -1, 0)
    far_a = step(before[:1], 1, 0)
    far_b = step(after[1:], -1, 0)
    line = jnp.concatenate([gated, after, far_a, far_b, before], axis=0)
    arrived, line = lax.optimization_barrier((arrived, line))

    def exchange(value, groups):
        return lax.all_to_all(
            value, ("c", "tp"), 0, 0, axis_index_groups=groups, tiled=True
        )

    def spread(value, groups):
        return exchange(jnp.broadcast_to(value[None], (side,) + value.shape), groups)

    rows_own = arrived[:, 0].reshape(half, cols_part)
    rows_other = lax.ppermute(arrived[:, 1].reshape(half, cols_part), "c", swap)
    rows = jnp.concatenate([rows_own, rows_other], axis=0)
    x = spread(spread(rows, early), late).reshape(tp, slot_total, cols_part)
    weights = (expert_gate[0], expert_up[0], expert_down[0])
    part = expert_part(me, x, *weights, rows_b)
    part = part.reshape(side, side, slot_total, cols_part)
    half_sums = sum_parts(exchange(part, early))
    half_sums, line = lax.optimization_barrier((half_sums, line))
    line_before = step(line, 1, 1)
    line_after = step(line, -1, 1)
    expert_rows = exchange(half_sums, late)
    expert_rows = sum_parts(expert_rows)
    back_own = expert_rows[:half]
    back_other = lax.ppermute(expert_rows[half:], "c", swap)
    back = jnp.stack(
        [
            back_own.reshape(depth, capacity, cols_part),
            back_other.reshape(depth, capacity, cols_part),
        ],
        axis=1,
    )
    back, near_a, near_b = lax.optimization_barrier((back, line_before[:4], line_after[4:]))
    line_far_a = step(near_a, 1, 1)
    line_far_b = step(near_b, -1, 1)
    returned = lax.all_to_all(back, "z", 0, 0, tiled=True)
    mixed_out = mixer_product(
        me,
        (line, line_after, line_far_a, line_far_b, line_before),
        mixer_proj.reshape(tp, width_part, cols_part),
        length // 4,
    )
    returned, mixed_out = lax.optimization_barrier((returned, mixed_out))
    returned = returned.reshape(slot_total, cols_part)
    picked0 = jnp.dot(pick0.astype(BF), returned, preferred_element_type=F32)
    picked1 = jnp.dot(pick1.astype(BF), returned, preferred_element_type=F32)
    expert_out = (
        picked0 * route_weights[:, 0:1] + picked1 * route_weights[:, 1:2]
    ).astype(BF)

    return (mixed_out, expert_out)


def solution(mesh):
    ep, tp = mesh.devices.shape
    fine = Mesh(mesh.devices.reshape(ep // 2, 2, tp), ("z", "c", "tp"))
    both = ("z", "c")
    return jax.shard_map(
        layer,
        mesh=fine,
        in_specs=(
            P("tp", both),
            P("tp", both),
            P("tp", both),
            P(),
            P(None, "tp"),
            P(both, "tp"),
            P(both, None),
            P(both, None),
            P(both, None, "tp"),
            P(both, None, "tp"),
            P(both, "tp", None),
        ),
        out_specs=(P(both, "tp"), P(both, "tp")),
        check_vma=False,
    )
```

profile of v0, /device:TPU:24, one launch (start us, length us, event | category | flops | bytes accessed | tf_op | source)
XLA Modules:
  0.0 202.5 jit_solution(17743113467906483827)
XLA Ops:
  8.9 3.4 %collective-permute-start.2 = (bf16[2,32,2048]{2,1,0:T(8,128)(2,1)S(1)}, bf16[2,32,2048]{2,1,0:T(8,128)(2,1)S(1)}, u32[]{:S(2)}, u32[]{:S(2)}) collective-permute-start(bf16[2,32,2048]{2,1,0:T(8,128)(2,1)S(1)} %bitcast.40), channel_id=1, source_target_pairs={{0,1},{1,2},{2,3},{3,0},{4,5},{5,6},{6,7},{7,4},{8,9},{9,10},{10,1... | collective-permute-start | bytes 786440 | tf_op jit(solution)/shard_map/ppermute | solution.py:195
  12.3 3.7 %collective-permute-start.1 = (bf16[2,32,2048]{2,1,0:T(8,128)(2,1)S(1)}, bf16[2,32,2048]{2,1,0:T(8,128)(2,1)S(1)}, u32[]{:S(2)}, u32[]{:S(2)}) collective-permute-start(bf16[2,32,2048]{2,1,0:T(8,128)(2,1)S(1)} %bitcast.41), channel_id=1, source_target_pairs={{0,3},{1,0},{2,1},{3,2},{4,7},{5,4},{6,5},{7,6},{8,11},{9,8},{10,9... | collective-permute-start | bytes 786440 | tf_op jit(solution)/shard_map/ppermute | solution.py:195
  16.0 18.9 %all-to-all-start = ((bf16[16,2,32,128]{3,2,1,0:T(8,128)(2,1)}), bf16[16,2,32,128]{3,2,1,0:T(8,128)(2,1)S(1)}, u32[]{:S(2)}, u32[]{:S(2)}) async-start(bf16[16,2,32,128]{3,2,1,0:T(8,128)(2,1)} %bitcast.7), calls=%async_computation | async-start | bytes 524288 | tf_op jit(solution)/shard_map/all_to_all | solution.py:159
  34.9 2.2 %collective-permute-start.3 = (bf16[1,32,2048]{2,1,0:T(8,128)(2,1)S(1)}, bf16[1,32,2048]{2,1,0:T(8,128)(2,1)S(1)}, u32[]{:S(2)}, u32[]{:S(2)}) collective-permute-start(bf16[1,32,2048]{2,1,0:T(8,128)(2,1)S(1)} %slice.82), channel_id=1, source_target_pairs={{0,1},{1,2},{2,3},{3,0},{4,5},{5,6},{6,7},{7,4},{8,9},{9,10},{10,1... | collective-permute-start | bytes 393224 | tf_op jit(solution)/shard_map/ppermute | solution.py:195
  37.2 4.9 %collective-permute-start.4 = (bf16[1,32,2048]{2,1,0:T(8,128)(2,1)S(1)}, bf16[1,32,2048]{2,1,0:T(8,128)(2,1)S(1)}, u32[]{:S(2)}, u32[]{:S(2)}) collective-permute-start(bf16[1,32,2048]{2,1,0:T(8,128)(2,1)S(1)} %slice.83), channel_id=1, source_target_pairs={{0,3},{1,0},{2,1},{3,2},{4,7},{5,4},{6,5},{7,6},{8,11},{9,8},{10,9... | collective-permute-start | bytes 393224 | tf_op jit(solution)/shard_map/ppermute | solution.py:195
  44.6 6.7 %all-to-all-done = bf16[16,2,32,128]{3,2,1,0:T(8,128)(2,1)S(1)} async-done(((bf16[16,2,32,128]{3,2,1,0:T(8,128)(2,1)}), bf16[16,2,32,128]{3,2,1,0:T(8,128)(2,1)S(1)}, u32[]{:S(2)}, u32[]{:S(2)}) %all-to-all-start) | async-done | bytes 262176 | tf_op jit(solution)/shard_map/all_to_all | solution.py:159
  54.7 13.8 %all_to_all.30 = bf16[4,1024,128]{2,1,0:T(8,128)(2,1)S(1)} all-to-all(bf16[4,1024,128]{2,1,0:T(8,128)(2,1)S(1)} %broadcast_in_dim.10), channel_id=1, replica_groups={{0,1,2,3},{4,5,6,7},{8,9,10,11},{12,13,14,15},{16,20,24,28},{17,21,25,2..., dimensions={0} | all-to-all | bytes 2097152 | tf_op jit(solution)/shard_map/all_to_all | solution.py:206
  68.5 2.8 %broadcast_in_dim.11 = bf16[4,4,1024,128]{3,2,1,0:T(8,128)(2,1)} broadcast(bf16[4,1024,128]{2,1,0:T(8,128)(2,1)S(1)} %all_to_all.30), dimensions={1,2,3} | broadcast | bytes 5242880 | tf_op jit(solution)/shard_map/broadcast_in_dim | solution.py:211
  71.3 5.9 %all-to-all-start.2 = ((bf16[4,4,1024,128]{3,2,1,0:T(8,128)(2,1)}), bf16[4,4,1024,128]{3,2,1,0:T(8,128)(2,1)}, u32[]{:S(2)}, u32[]{:S(2)}) async-start(bf16[4,4,1024,128]{3,2,1,0:T(8,128)(2,1)} %broadcast_in_dim.11), calls=%async_computation.2 | async-start | bytes 8388608 | tf_op jit(solution)/shard_map/all_to_all | solution.py:206
  77.3 25.8 %all-to-all-done.2 = bf16[4,4,1024,128]{3,2,1,0:T(8,128)(2,1)} async-done(((bf16[4,4,1024,128]{3,2,1,0:T(8,128)(2,1)}), bf16[4,4,1024,128]{3,2,1,0:T(8,128)(2,1)}, u32[]{:S(2)}, u32[]{:S(2)}) %all-to-all-start.2) | async-done | bytes 4194336 | tf_op jit(solution)/shard_map/all_to_all | solution.py:206
  104.3 6.0 %shard_map.122 = bf16[16,1024,128]{2,1,0:T(8,128)(2,1)S(1)} custom-call(s32[1]{0:T(128)} %bitcast.me_ref, bf16[16,1024,128]{2,1,0:T(8,128)(2,1)} %bitcast.14.x_ref, bf16[2048,256]{1,0:T(8,128)(2,1)S(1)} %bitcast.37, bf16[2048,256]{1,0:T(8,128)(2,1)S(1)} %bitcast.38, bf16[256,2048]{1,0:T(8,128)(2,1)S(1)} %bitcast.39), custom_call_target="tpu_custom_call" | custom-call | flops 3221225472 | bytes 11534336 | tf_op jit(solution)/shard_map/pallas_call | solution.py:39
  110.2 31.2 %all_to_all.31 = bf16[4,4,1024,128]{3,2,1,0:T(8,128)(2,1)} all-to-all(bf16[4,4,1024,128]{3,2,1,0:T(8,128)(2,1)S(1)} %bitcast.35), channel_id=1, replica_groups={{0,1,2,3},{4,5,6,7},{8,9,10,11},{12,13,14,15},{16,20,24,28},{17,21,25,2..., dimensions={0} | all-to-all | bytes 8388608 | tf_op jit(solution)/shard_map/all_to_all | solution.py:206
  141.4 4.2 %reduce_sum.50 = bf16[4,1024,128]{2,1,0:T(8,128)(2,1)} reduce(bf16[4,4,1024,128]{3,2,1,0:T(8,128)(2,1)} %all_to_all.31, bf16[]{:T(256)} %constant.22.clone.1), dimensions={0}, to_apply=%region_2.3 | reduce | flops 1572864 | bytes 5242882 | tf_op jit(solution)/shard_map/reduce_sum | solution.py:113
  145.6 6.4 %all-to-all-start.4 = ((bf16[4,1024,128]{2,1,0:T(8,128)(2,1)}), bf16[4,1024,128]{2,1,0:T(8,128)(2,1)}, u32[]{:S(2)}, u32[]{:S(2)}) async-start(bf16[4,1024,128]{2,1,0:T(8,128)(2,1)} %reduce_sum.50), calls=%async_computation.4 | async-start | bytes 2097152 | tf_op jit(solution)/shard_map/all_to_all | solution.py:206
  152.0 2.0 collective-permute-start.7
  153.9 3.9 %collective-permute-start.8 = (bf16[8,32,2048]{2,1,0:T(8,128)(2,1)S(1)}, bf16[8,32,2048]{2,1,0:T(8,128)(2,1)S(1)}, u32[]{:S(2)}, u32[]{:S(2)}) collective-permute-start(bf16[8,32,2048]{2,1,0:T(8,128)(2,1)S(1)} %constant_dynamic-update-slice_fusion.y0_ref), channel_id=1, source_target_pairs={{0,12},{1,13},{2,14},{3,15},{4,0},{5,1},{6,2},{7,3},{8,4},{9,5},{1... | collective-permute-start | bytes 3145736 | tf_op jit(solution)/shard_map/ppermute | solution.py:195
  157.8 3.1 %all-to-all-done.4 = bf16[4,1024,128]{2,1,0:T(8,128)(2,1)} async-done(((bf16[4,1024,128]{2,1,0:T(8,128)(2,1)}), bf16[4,1024,128]{2,1,0:T(8,128)(2,1)}, u32[]{:S(2)}, u32[]{:S(2)}) %all-to-all-start.4) | async-done | bytes 1048608 | tf_op jit(solution)/shard_map/all_to_all | solution.py:206
  160.9 2.1 %reduce_sum.51 = bf16[1024,128]{1,0:T(8,128)(2,1)} reduce(bf16[4,1024,128]{2,1,0:T(8,128)(2,1)} %all-to-all-done.4, bf16[]{:T(256)} %constant.22.clone.1), dimensions={0}, to_apply=%region_3.4 | reduce | flops 393216 | bytes 1310722 | tf_op jit(solution)/shard_map/reduce_sum | solution.py:113
  168.0 3.4 %collective-permute-done.7.y3_ref = bf16[8,32,2048]{2,1,0:T(8,128)(2,1)S(1)} collective-permute-done((bf16[8,32,2048]{2,1,0:T(8,128)(2,1)S(1)}, bf16[8,32,2048]{2,1,0:T(8,128)(2,1)S(1)}, u32[]{:S(2)}, u32[]{:S(2)}) %collective-permute-start.7) | collective-permute-done | bytes 1048608 | tf_op jit(solution)/shard_map/ppermute | solution.py:195
  173.1 6.4 %all-to-all-start.5 = ((bf16[16,2,32,128]{3,2,1,0:T(8,128)(2,1)}), bf16[16,2,32,128]{3,2,1,0:T(8,128)(2,1)}, u32[]{:S(2)}, u32[]{:S(2)}) async-start(bf16[16,2,32,128]{3,2,1,0:T(8,128)(2,1)} %pad_maximum_fusion.1), calls=%async_computation.5 | async-start | bytes 524288 | tf_op jit(solution)/shard_map/all_to_all | solution.py:238
  179.6 4.2 %collective-permute-start.9 = (bf16[4,32,2048]{2,1,0:T(8,128)(2,1)}, bf16[4,32,2048]{2,1,0:T(8,128)(2,1)S(1)}, u32[]{:S(2)}, u32[]{:S(2)}) collective-permute-start(bf16[4,32,2048]{2,1,0:T(8,128)(2,1)} %slice.86), channel_id=1, source_target_pairs={{0,4},{1,5},{2,6},{3,7},{4,8},{5,9},{6,10},{7,11},{8,12},{9,13},{1... | collective-permute-start | bytes 1572872 | tf_op jit(solution)/shard_map/ppermute | solution.py:195
  185.8 5.1 %collective-permute-done.9.y2a_ref = bf16[4,32,2048]{2,1,0:T(8,128)(2,1)S(1)} collective-permute-done((bf16[4,32,2048]{2,1,0:T(8,128)(2,1)}, bf16[4,32,2048]{2,1,0:T(8,128)(2,1)S(1)}, u32[]{:S(2)}, u32[]{:S(2)}) %collective-permute-start.9) | collective-permute-done | bytes 524320 | tf_op jit(solution)/shard_map/ppermute | solution.py:195
  190.9 5.5 %collective-permute-done.10.y2b_ref = bf16[4,32,2048]{2,1,0:T(8,128)(2,1)S(1)} collective-permute-done((bf16[4,32,2048]{2,1,0:T(8,128)(2,1)}, bf16[4,32,2048]{2,1,0:T(8,128)(2,1)S(1)}, u32[]{:S(2)}, u32[]{:S(2)}) %collective-permute-start.10) | collective-permute-done | bytes 524320 | tf_op jit(solution)/shard_map/ppermute | solution.py:195
  196.3 2.9 %shard_map.123 = bf16[2048,128]{1,0:T(8,128)(2,1)} custom-call(s32[1]{0:T(128)} %bitcast.me_ref, bf16[8,32,2048]{2,1,0:T(8,128)(2,1)S(1)} %constant_dynamic-update-slice_fusion.y0_ref, bf16[8,32,2048]{2,1,0:T(8,128)(2,1)S(1)} %collective-permute-done.8.y1_ref, bf16[4,32,2048]{2,1,0:T(8,128)(2,1)S(1)} %collective-permute-done.9.y2a_ref, ...), custom_call_target="tpu_custom_call" | custom-call | flops 536870912 | bytes 4980736 | tf_op jit(solution)/shard_map/pallas_call | solution.py:91
  (52 shorter events, 27.2 us)
Async XLA Ops:
  0.6 1.8 copy-start
  4.9 2.6 %collective-permute-start = (bf16[64,2]{1,0:T(8,128)(2,1)S(1)}, bf16[64,2]{1,0:T(8,128)(2,1)S(1)}, u32[]{:S(2)}, u32[]{:S(2)}) collective-permute-start(bf16[64,2]{1,0:T(8,128)(2,1)S(1)} %slice.78), channel_id=1, source_target_pairs={{0,16},{16,32},{32,48},{48,64},{64,80},{80,96},{96,112},{112,128},... | collective-permute-start | bytes 776 | tf_op jit(solution)/shard_map/ppermute | solution.py:169
  8.9 26.0 %collective-permute-start.2 = (bf16[2,32,2048]{2,1,0:T(8,128)(2,1)S(1)}, bf16[2,32,2048]{2,1,0:T(8,128)(2,1)S(1)}, u32[]{:S(2)}, u32[]{:S(2)}) collective-permute-start(bf16[2,32,2048]{2,1,0:T(8,128)(2,1)S(1)} %bitcast.40), channel_id=1, source_target_pairs={{0,1},{1,2},{2,3},{3,0},{4,5},{5,6},{6,7},{7,4},{8,9},{9,10},{10,1... | collective-permute-start | bytes 786440 | tf_op jit(solution)/shard_map/ppermute | solution.py:195
  12.3 24.8 %collective-permute-start.1 = (bf16[2,32,2048]{2,1,0:T(8,128)(2,1)S(1)}, bf16[2,32,2048]{2,1,0:T(8,128)(2,1)S(1)}, u32[]{:S(2)}, u32[]{:S(2)}) collective-permute-start(bf16[2,32,2048]{2,1,0:T(8,128)(2,1)S(1)} %bitcast.41), channel_id=1, source_target_pairs={{0,3},{1,0},{2,1},{3,2},{4,7},{5,4},{6,5},{7,6},{8,11},{9,8},{10,9... | collective-permute-start | bytes 786440 | tf_op jit(solution)/shard_map/ppermute | solution.py:195
  16.0 35.4 %all-to-all-start = ((bf16[16,2,32,128]{3,2,1,0:T(8,128)(2,1)}), bf16[16,2,32,128]{3,2,1,0:T(8,128)(2,1)S(1)}, u32[]{:S(2)}, u32[]{:S(2)}) async-start(bf16[16,2,32,128]{3,2,1,0:T(8,128)(2,1)} %bitcast.7), calls=%async_computation | async-start | bytes 524288 | tf_op jit(solution)/shard_map/all_to_all | solution.py:159
  34.9 8.1 %collective-permute-start.3 = (bf16[1,32,2048]{2,1,0:T(8,128)(2,1)S(1)}, bf16[1,32,2048]{2,1,0:T(8,128)(2,1)S(1)}, u32[]{:S(2)}, u32[]{:S(2)}) collective-permute-start(bf16[1,32,2048]{2,1,0:T(8,128)(2,1)S(1)} %slice.82), channel_id=1, source_target_pairs={{0,1},{1,2},{2,3},{3,0},{4,5},{5,6},{6,7},{7,4},{8,9},{9,10},{10,1... | collective-permute-start | bytes 393224 | tf_op jit(solution)/shard_map/ppermute | solution.py:195
  37.2 7.4 %collective-permute-start.4 = (bf16[1,32,2048]{2,1,0:T(8,128)(2,1)S(1)}, bf16[1,32,2048]{2,1,0:T(8,128)(2,1)S(1)}, u32[]{:S(2)}, u32[]{:S(2)}) collective-permute-start(bf16[1,32,2048]{2,1,0:T(8,128)(2,1)S(1)} %slice.83), channel_id=1, source_target_pairs={{0,3},{1,0},{2,1},{3,2},{4,7},{5,4},{6,5},{7,6},{8,11},{9,8},{10,9... | collective-permute-start | bytes 393224 | tf_op jit(solution)/shard_map/ppermute | solution.py:195
  51.3 3.2 %collective-permute-start.5 = (bf16[512,128]{1,0:T(8,128)(2,1)S(1)}, bf16[512,128]{1,0:T(8,128)(2,1)S(1)}, u32[]{:S(2)}, u32[]{:S(2)}) collective-permute-start(bf16[512,128]{1,0:T(8,128)(2,1)S(1)} %bitcast.45), channel_id=1, source_target_pairs={{0,16},{16,0},{1,17},{17,1},{2,18},{18,2},{3,19},{19,3},{4,20},{20... | collective-permute-start | bytes 393224 | tf_op jit(solution)/shard_map/ppermute | solution.py:214
  71.3 31.7 %copy-start.2 = (bf16[1,2048,256]{2,1,0:T(8,128)(2,1)S(1)}, bf16[1,2048,256]{2,1,0:T(8,128)(2,1)}, u32[]{:S(2)}) copy-start(bf16[1,2048,256]{2,1,0:T(8,128)(2,1)} %param.19) | copy-start | bytes 3145732
  71.3 31.7 %copy-start.3 = (bf16[1,2048,256]{2,1,0:T(8,128)(2,1)S(1)}, bf16[1,2048,256]{2,1,0:T(8,128)(2,1)}, u32[]{:S(2)}) copy-start(bf16[1,2048,256]{2,1,0:T(8,128)(2,1)} %param.20) | copy-start | bytes 3145732
  71.3 31.7 %all-to-all-start.2 = ((bf16[4,4,1024,128]{3,2,1,0:T(8,128)(2,1)}), bf16[4,4,1024,128]{3,2,1,0:T(8,128)(2,1)}, u32[]{:S(2)}, u32[]{:S(2)}) async-start(bf16[4,4,1024,128]{3,2,1,0:T(8,128)(2,1)} %broadcast_in_dim.11), calls=%async_computation.2 | async-start | bytes 8388608 | tf_op jit(solution)/shard_map/all_to_all | solution.py:206
  103.0 1.2 copy-start.4
  145.6 40.2 %copy-start.5 = (f32[256,2]{0,1:T(2,128)S(1)}, f32[256,2]{0,1:T(2,128)}, u32[]{:S(2)}) copy-start(f32[256,2]{0,1:T(2,128)} %param.18) | copy-start | bytes 6148
  145.6 50.7 %copy-start.1 = (bf16[1024,128]{1,0:T(8,128)(2,1)S(1)}, bf16[1024,128]{1,0:T(8,128)(2,1)}, u32[]{:S(2)}) copy-start(bf16[1024,128]{1,0:T(8,128)(2,1)} %param.15) | copy-start | bytes 786436
  145.6 15.3 %all-to-all-start.4 = ((bf16[4,1024,128]{2,1,0:T(8,128)(2,1)}), bf16[4,1024,128]{2,1,0:T(8,128)(2,1)}, u32[]{:S(2)}, u32[]{:S(2)}) async-start(bf16[4,1024,128]{2,1,0:T(8,128)(2,1)} %reduce_sum.50), calls=%async_computation.4 | async-start | bytes 2097152 | tf_op jit(solution)/shard_map/all_to_all | solution.py:206
  152.0 19.5 %collective-permute-start.7 = (bf16[8,32,2048]{2,1,0:T(8,128)(2,1)S(1)}, bf16[8,32,2048]{2,1,0:T(8,128)(2,1)S(1)}, u32[]{:S(2)}, u32[]{:S(2)}) collective-permute-start(bf16[8,32,2048]{2,1,0:T(8,128)(2,1)S(1)} %constant_dynamic-update-slice_fusion.y0_ref), channel_id=1, source_target_pairs={{0,4},{1,5},{2,6},{3,7},{4,8},{5,9},{6,10},{7,11},{8,12},{9,13},{1... | collective-permute-start | bytes 3145736 | tf_op jit(solution)/shard_map/ppermute | solution.py:195
  153.9 18.4 %collective-permute-start.8 = (bf16[8,32,2048]{2,1,0:T(8,128)(2,1)S(1)}, bf16[8,32,2048]{2,1,0:T(8,128)(2,1)S(1)}, u32[]{:S(2)}, u32[]{:S(2)}) collective-permute-start(bf16[8,32,2048]{2,1,0:T(8,128)(2,1)S(1)} %constant_dynamic-update-slice_fusion.y0_ref), channel_id=1, source_target_pairs={{0,12},{1,13},{2,14},{3,15},{4,0},{5,1},{6,2},{7,3},{8,4},{9,5},{1... | collective-permute-start | bytes 3145736 | tf_op jit(solution)/shard_map/ppermute | solution.py:195
  164.1 3.2 %collective-permute-start.6 = (bf16[512,128]{1,0:T(8,128)(2,1)S(1)}, bf16[512,128]{1,0:T(8,128)(2,1)S(1)}, u32[]{:S(2)}, u32[]{:S(2)}) collective-permute-start(bf16[512,128]{1,0:T(8,128)(2,1)S(1)} %get-tuple-element.29), channel_id=1, source_target_pairs={{0,16},{16,0},{1,17},{17,1},{2,18},{18,2},{3,19},{19,3},{4,20},{20... | collective-permute-start | bytes 393224 | tf_op jit(solution)/shard_map/ppermute | solution.py:227
  173.1 26.1 %all-to-all-start.5 = ((bf16[16,2,32,128]{3,2,1,0:T(8,128)(2,1)}), bf16[16,2,32,128]{3,2,1,0:T(8,128)(2,1)}, u32[]{:S(2)}, u32[]{:S(2)}) async-start(bf16[16,2,32,128]{3,2,1,0:T(8,128)(2,1)} %pad_maximum_fusion.1), calls=%async_computation.5 | async-start | bytes 524288 | tf_op jit(solution)/shard_map/all_to_all | solution.py:238
  179.6 11.3 %collective-permute-start.9 = (bf16[4,32,2048]{2,1,0:T(8,128)(2,1)}, bf16[4,32,2048]{2,1,0:T(8,128)(2,1)S(1)}, u32[]{:S(2)}, u32[]{:S(2)}) collective-permute-start(bf16[4,32,2048]{2,1,0:T(8,128)(2,1)} %slice.86), channel_id=1, source_target_pairs={{0,4},{1,5},{2,6},{3,7},{4,8},{5,9},{6,10},{7,11},{8,12},{9,13},{1... | collective-permute-start | bytes 1572872 | tf_op jit(solution)/shard_map/ppermute | solution.py:195
  183.8 12.5 %collective-permute-start.10 = (bf16[4,32,2048]{2,1,0:T(8,128)(2,1)}, bf16[4,32,2048]{2,1,0:T(8,128)(2,1)S(1)}, u32[]{:S(2)}, u32[]{:S(2)}) collective-permute-start(bf16[4,32,2048]{2,1,0:T(8,128)(2,1)} %slice.87), channel_id=1, source_target_pairs={{0,12},{1,13},{2,14},{3,15},{4,0},{5,1},{6,2},{7,3},{8,4},{9,5},{1... | collective-permute-start | bytes 1572872 | tf_op jit(solution)/shard_map/ppermute | solution.py:195
where the time goes:
time: 204 us; the launch traced here: 203 us
  starting transfers between devices  69.3 us (34%)
  waiting for transfers between devices  54.8 us (27%)
  blocking collectives  45 us (22%)
  other arithmetic  10.4 us (5%)
  Pallas kernels  8.89 us (4%)
  local copies, waits for them, and re-layouts  8.55 us (4%)
  matrix products  4.74 us (2%)
    all_to_all x2, blocking collectives, exchange(): lax.all_to_all(value, ('c', 'tp'), 0, 0, axis_index_groups=groups, tiled=...  45 us
    all_to_all x2, waiting for transfers between devices, exchange(): lax.all_to_all(value, ('c', 'tp'), 0, 0, axis_index_groups=groups, tiled=...  28.9 us
    ppermute x8, starting transfers between devices, step(): return lax.ppermute(value, ('c', 'tp'), pairs)  26.1 us
    all_to_all x1, starting transfers between devices, layer(): lax.all_to_all(outgoing.reshape(depth, 2, capacity, cols_part), 'z', 0, 0...  18.9 us
    ppermute x8, waiting for transfers between devices, step(): return lax.ppermute(value, ('c', 'tp'), pairs)  16.5 us
    all_to_all x2, starting transfers between devices, exchange(): lax.all_to_all(value, ('c', 'tp'), 0, 0, axis_index_groups=groups, tiled=...  12.3 us
    all_to_all x1, waiting for transfers between devices, layer(): lax.all_to_all(outgoing.reshape(depth, 2, capacity, cols_part), 'z', 0, 0...  6.75 us
    all_to_all x1, starting transfers between devices, layer(): returned = lax.all_to_all(back, 'z', 0, 0, tiled=True)  6.42 us
  transfers between devices with their start and end apart: 15, of which 11 were waited for; matrix products, arithmetic and copies ran while one was open for 3% of the time, Pallas kernels for 1%

commit v1 on v0

--- a/solution.py
+++ b/solution.py
@@ -1,3 +1,5 @@
+import functools
+
 import jax
 import jax.numpy as jnp
 from jax import lax
@@ -12,6 +14,57 @@
 F32 = jnp.float32
 
 
+def ones_where(test):
+    return jnp.where(test, 1.0, 0.0).astype(BF)
+
+
+def dispatch_kernel(me_ref, routes_ref, rows_ref, places_ref, out_ref, *, experts, tp):
+    core = me_ref[0] // tp
+    rows = rows_ref.shape[0]
+    slot_total = out_ref.shape[0]
+    capacity = slot_total // experts
+    ids = lax.broadcasted_iota(jnp.int32, (rows, experts), 1)
+    named = [routes_ref[:, k : k + 1] for k in range(2)]
+    hit = [n == ids for n in named]
+    later = lax.broadcasted_iota(jnp.int32, (rows, rows), 0)
+    sooner = lax.broadcasted_iota(jnp.int32, (rows, rows), 1)
+    earlier = jnp.dot(
+        ones_where(sooner < later), ones_where(hit[0] | hit[1]), preferred_element_type=F32
+    )
+    slots = lax.broadcasted_iota(jnp.int32, (rows, slot_total), 1)
+    taken = []
+    for k in range(2):
+        slot = jnp.sum(jnp.where(hit[k], earlier, 0.0), axis=1, keepdims=True)
+        place = (named[k] ^ core) * capacity + slot.astype(jnp.int32)
+        places_ref[:, k : k + 1] = place
+        taken.append(place == slots)
+    out_ref[...] = lax.dot_general(
+        ones_where(taken[0] | taken[1]),
+        rows_ref[...],
+        (((0,), (0,)), ((), ())),
+        preferred_element_type=F32,
+    ).astype(BF)
+
+
+def combine_kernel(places_ref, weights_ref, returned_ref, out_ref):
+    rows = out_ref.shape[0]
+    slots = lax.broadcasted_iota(jnp.int32, (rows, returned_ref.shape[0]), 1)
+    total = None
+    for k in range(2):
+        pick = ones_where(places_ref[:, k : k + 1] == slots)
+        picked = jnp.dot(pick, returned_ref[...], preferred_element_type=F32)
+        term = picked * weights_ref[:, k : k + 1]
+        total = term if total is None else total + term
+    out_ref[...] = total.astype(BF)
+
+
+def sum_kernel(in_ref, out_ref):
+    total = in_ref[0].astype(F32)
+    for j in range(1, in_ref.shape[0]):
+        total = total + in_ref[j].astype(F32)
+    out_ref[...] = total.astype(BF)
+
+
 def expert_kernel(me_ref, x_ref, gate_ref, up_ref, down_ref, out_ref):
     parts = x_ref.shape[0]
     cols = x_ref.shape[2]
@@ -19,9 +72,8 @@
     core = me_ref[0] // parts
     natural = [j for j in range(parts)]
     turned = [(j % side) * side + j // side for j in range(parts)]
-    load = [jnp.where(core == 0, natural[j], turned[j]) for j in range(parts)]
     store = [jnp.where(core == 0, turned[j], natural[j]) for j in range(parts)]
-    x = jnp.concatenate([x_ref[load[j]] for j in range(parts)], axis=1)
+    x = jnp.concatenate([x_ref[j] for j in range(parts)], axis=1)
     values = x.astype(F32)
     squares = jnp.sum(values * values, axis=1, keepdims=True)
     scale = lax.rsqrt(squares / (parts * cols) + EPSILON)
@@ -109,8 +161,16 @@
     )(me.reshape(1), *pieces, proj)
 
 
-def sum_parts(arrived):
-    return arrived.astype(F32).sum(axis=0).astype(BF)
+def sum_parts(arrived, steps):
+    parts, rows, cols = arrived.shape
+    return pl.pallas_call(
+        sum_kernel,
+        grid=(steps,),
+        in_specs=[pl.BlockSpec((parts, rows // steps, cols), lambda i: (0, i, 0))],
+        out_specs=pl.BlockSpec((rows // steps, cols), lambda i: (i, 0)),
+        out_shape=jax.ShapeDtypeStruct((rows, cols), BF),
+        compiler_params=pltpu.CompilerParams(vmem_limit_bytes=12 * 1024 * 1024),
+    )(arrived)
 
 
 def layer(
@@ -129,32 +189,32 @@
     depth = lax.axis_size("z")
     experts = 2 * depth
     tp = lax.axis_size("tp")
-    core = lax.axis_index("c")
     me = lax.axis_index(("c", "tp"))
     rows_b, cols_part = token_rows.shape
     capacity = 4 * rows_b // experts
     slot_total = experts * capacity
     half = slot_total // 2
 
-    expert_ids = jnp.arange(experts, dtype=jnp.int32)[None, :]
-    hit0 = routes[:, 0:1] == expert_ids
-    hit1 = routes[:, 1:2] == expert_ids
-    hits = (hit0 | hit1).astype(BF)
-    order = jnp.arange(rows_b, dtype=jnp.int32)
-    earlier_rows = (order[None, :] < order[:, None]).astype(BF)
-    earlier = jnp.dot(earlier_rows, hits, preferred_element_type=F32).astype(jnp.int32)
-    places = []
-    for k, hit in enumerate((hit0, hit1)):
-        slot = jnp.sum(jnp.where(hit, earlier, 0), axis=1)
-        places.append((routes[:, k] ^ core) * capacity + slot)
-    slot_ids = jnp.arange(slot_total, dtype=jnp.int32)[None, :]
-    pick0 = places[0][:, None] == slot_ids
-    pick1 = places[1][:, None] == slot_ids
-    pick_any = (pick0 | pick1).astype(BF)
-    outgoing = lax.dot_general(
-        pick_any, token_rows, (((0,), (0,)), ((), ())), preferred_element_type=F32
-    ).astype(BF)
-
+    places, outgoing = pl.pallas_call(
+        functools.partial(dispatch_kernel, experts=experts, tp=tp),
+        grid_spec=pltpu.PrefetchScalarGridSpec(
+            num_scalar_prefetch=1,
+            grid=(1,),
+            in_specs=[
+                pl.BlockSpec(routes.shape, lambda i, c: (0, 0)),
+                pl.BlockSpec(token_rows.shape, lambda i, c: (0, 0)),
+            ],
+            out_specs=[
+                pl.BlockSpec(routes.shape, lambda i, c: (0, 0)),
+                pl.BlockSpec((slot_total, cols_part), lambda i, c: (0, 0)),
+            ],
+        ),
+        out_shape=[
+            jax.ShapeDtypeStruct(routes.shape, jnp.int32),
+            jax.ShapeDtypeStruct((slot_total, cols_part), BF),
+        ],
+        compiler_params=pltpu.CompilerParams(vmem_limit_bytes=12 * 1024 * 1024),
+    )(me.reshape(1), routes, token_rows)
     outgoing, conv_input, in_gate = lax.optimization_barrier((outgoing, conv_input, in_gate))
     arrived = lax.all_to_all(
         outgoing.reshape(depth, 2, capacity, cols_part), "z", 0, 0, tiled=True
@@ -197,9 +257,8 @@
     gated = gated.reshape(2, width_part // 2, length)
     before = step(gated, 1, 0)
     after = step(gated, -1, 0)
-    far_a = step(before[:1], 1, 0)
-    far_b = step(after[1:], -1, 0)
-    line = jnp.concatenate([gated, after, far_a, far_b, before], axis=0)
+    far = step(gated, 2, 0)
+    line = jnp.concatenate([gated, after, far, before], axis=0)
     arrived, line = lax.optimization_barrier((arrived, line))
 
     def exchange(value, groups):
@@ -207,22 +266,22 @@
             value, ("c", "tp"), 0, 0, axis_index_groups=groups, tiled=True
         )
 
-    def spread(value, groups):
-        return exchange(jnp.broadcast_to(value[None], (side,) + value.shape), groups)
-
     rows_own = arrived[:, 0].reshape(half, cols_part)
     rows_other = lax.ppermute(arrived[:, 1].reshape(half, cols_part), "c", swap)
     rows = jnp.concatenate([rows_own, rows_other], axis=0)
-    x = spread(spread(rows, early), late).reshape(tp, slot_total, cols_part)
+    x = lax.all_to_all(
+        jnp.broadcast_to(rows[None], (tp,) + rows.shape), "tp", 0, 0, tiled=True
+    )
     weights = (expert_gate[0], expert_up[0], expert_down[0])
     part = expert_part(me, x, *weights, rows_b)
     part = part.reshape(side, side, slot_total, cols_part)
-    half_sums = sum_parts(exchange(part, early))
+    half_sums = exchange(part, early).reshape(side, side * slot_total, cols_part)
+    half_sums = sum_parts(half_sums, 8).reshape(side, slot_total, cols_part)
     half_sums, line = lax.optimization_barrier((half_sums, line))
     line_before = step(line, 1, 1)
     line_after = step(line, -1, 1)
     expert_rows = exchange(half_sums, late)
-    expert_rows = sum_parts(expert_rows)
+    expert_rows = sum_parts(expert_rows, 2)
     back_own = expert_rows[:half]
     back_other = lax.ppermute(expert_rows[half:], "c", swap)
     back = jnp.stack(
@@ -232,9 +291,8 @@
         ],
         axis=1,
     )
-    back, near_a, near_b = lax.optimization_barrier((back, line_before[:4], line_after[4:]))
-    line_far_a = step(near_a, 1, 1)
-    line_far_b = step(near_b, -1, 1)
+    line_far_a = step(line_before[:4], 1, 1)
+    line_far_b = step(line_after[4:], -1, 1)
     returned = lax.all_to_all(back, "z", 0, 0, tiled=True)
     mixed_out = mixer_product(
         me,
@@ -244,12 +302,11 @@
     )
     returned, mixed_out = lax.optimization_barrier((returned, mixed_out))
     returned = returned.reshape(slot_total, cols_part)
-    picked0 = jnp.dot(pick0.astype(BF), returned, preferred_element_type=F32)
-    picked1 = jnp.dot(pick1.astype(BF), returned, preferred_element_type=F32)
-    expert_out = (
-        picked0 * route_weights[:, 0:1] + picked1 * route_weights[:, 1:2]
-    ).astype(BF)
-
+    expert_out = pl.pallas_call(
+        combine_kernel,
+        out_shape=jax.ShapeDtypeStruct((rows_b, cols_part), BF),
+        compiler_params=pltpu.CompilerParams(vmem_limit_bytes=12 * 1024 * 1024),
+    )(places, route_weights, returned)
     return (mixed_out, expert_out)
 
 

time: 204 us -> 195 us (0.956)
  the two profiles are of different devices: /device:TPU:24 before, /device:TPU:1 now
where the time goes in v1:
time: 195 us; the launch traced here: 193 us
  blocking collectives  86.3 us (44%)
  starting transfers between devices  63 us (32%)
  waiting for transfers between devices  17.7 us (9%)
  Pallas kernels  15.2 us (8%)
  local copies, waits for them, and re-layouts  6.21 us (3%)
  other arithmetic  3.42 us (2%)
    all_to_all x1, blocking collectives, layer(): lax.all_to_all(jnp.broadcast_to(rows[None], (tp,) + rows.shape), 'tp', 0,...  56.9 us
    all_to_all x1, blocking collectives, exchange(): lax.all_to_all(value, ('c', 'tp'), 0, 0, axis_index_groups=groups, tiled=...  29.5 us
    ppermute x7, starting transfers between devices, step(): return lax.ppermute(value, ('c', 'tp'), pairs)  22.5 us
    all_to_all x1, starting transfers between devices, layer(): lax.all_to_all(outgoing.reshape(depth, 2, capacity, cols_part), 'z', 0, 0...  14 us
    ppermute x7, waiting for transfers between devices, step(): return lax.ppermute(value, ('c', 'tp'), pairs)  12.4 us
    all_to_all x1, starting transfers between devices, layer(): returned = lax.all_to_all(back, 'z', 0, 0, tiled=True)  9.78 us
    ppermute x1, starting transfers between devices, layer(): back_other = lax.ppermute(expert_rows[half:], 'c', swap)  5.66 us
    ppermute x1, starting transfers between devices, layer(): rim = lax.ppermute(z_rows[:, length - (KERNEL - 1):], ('z', 'c'), pairs)  4.91 us
  transfers between devices with their start and end apart: 13, of which 7 were waited for; matrix products, arithmetic and copies ran while one was open for 3% of the time, Pallas kernels for 2%

profile of v1, /device:TPU:1, one launch (start us, length us, event | category | flops | bytes accessed | tf_op | source)
XLA Modules:
  0.0 192.8 jit_solution(8780773331337181361)
XLA Ops:
  5.1 4.9 %collective-permute-start = (bf16[64,2]{1,0:T(8,128)(2,1)S(1)}, bf16[64,2]{1,0:T(8,128)(2,1)S(1)}, u32[]{:S(2)}, u32[]{:S(2)}) collective-permute-start(bf16[64,2]{1,0:T(8,128)(2,1)S(1)} %slice.52), channel_id=1, source_target_pairs={{0,16},{16,32},{32,48},{48,64},{64,80},{80,96},{96,112},{112,128},... | collective-permute-start | bytes 776 | tf_op jit(solution)/shard_map/ppermute | solution.py:229
  10.0 14.0 %all-to-all-start = ((bf16[16,2,32,128]{3,2,1,0:T(8,128)(2,1)}), bf16[16,2,32,128]{3,2,1,0:T(8,128)(2,1)S(1)}, u32[]{:S(2)}, u32[]{:S(2)}) async-start(bf16[16,2,32,128]{3,2,1,0:T(8,128)(2,1)} %bitcast.1), calls=%async_computation | async-start | bytes 524288 | tf_op jit(solution)/shard_map/all_to_all | solution.py:219
  25.6 4.6 %collective-permute-start.1 = (bf16[2,32,2048]{2,1,0:T(8,128)(2,1)S(1)}, bf16[2,32,2048]{2,1,0:T(8,128)(2,1)S(1)}, u32[]{:S(2)}, u32[]{:S(2)}) collective-permute-start(bf16[2,32,2048]{2,1,0:T(8,128)(2,1)S(1)} %bitcast.32), channel_id=1, source_target_pairs={{0,3},{1,0},{2,1},{3,2},{4,7},{5,4},{6,5},{7,6},{8,11},{9,8},{10,9... | collective-permute-start | bytes 786440 | tf_op jit(solution)/shard_map/ppermute | solution.py:255
  30.3 2.3 %collective-permute-start.2 = (bf16[2,32,2048]{2,1,0:T(8,128)(2,1)S(1)}, bf16[2,32,2048]{2,1,0:T(8,128)(2,1)S(1)}, u32[]{:S(2)}, u32[]{:S(2)}) collective-permute-start(bf16[2,32,2048]{2,1,0:T(8,128)(2,1)S(1)} %bitcast.33), channel_id=1, source_target_pairs={{0,2},{1,3},{2,0},{3,1},{4,6},{5,7},{6,4},{7,5},{8,10},{9,11},{10,... | collective-permute-start | bytes 786440 | tf_op jit(solution)/shard_map/ppermute | solution.py:255
  32.5 2.6 %collective-permute-start.3 = (bf16[2,32,2048]{2,1,0:T(8,128)(2,1)S(1)}, bf16[2,32,2048]{2,1,0:T(8,128)(2,1)S(1)}, u32[]{:S(2)}, u32[]{:S(2)}) collective-permute-start(bf16[2,32,2048]{2,1,0:T(8,128)(2,1)S(1)} %bitcast.34), channel_id=1, source_target_pairs={{0,1},{1,2},{2,3},{3,0},{4,5},{5,6},{6,7},{7,4},{8,9},{9,10},{10,1... | collective-permute-start | bytes 786440 | tf_op jit(solution)/shard_map/ppermute | solution.py:255
  35.1 4.0 %collective-permute-done.2 = bf16[2,32,2048]{2,1,0:T(8,128)(2,1)S(1)} collective-permute-done((bf16[2,32,2048]{2,1,0:T(8,128)(2,1)S(1)}, bf16[2,32,2048]{2,1,0:T(8,128)(2,1)S(1)}, u32[]{:S(2)}, u32[]{:S(2)}) %collective-permute-start.2) | collective-permute-done | bytes 262176 | tf_op jit(solution)/shard_map/ppermute | solution.py:255
  39.2 2.8 %collective-permute-done.3 = bf16[2,32,2048]{2,1,0:T(8,128)(2,1)S(1)} collective-permute-done((bf16[2,32,2048]{2,1,0:T(8,128)(2,1)S(1)}, bf16[2,32,2048]{2,1,0:T(8,128)(2,1)S(1)}, u32[]{:S(2)}, u32[]{:S(2)}) %collective-permute-start.3) | collective-permute-done | bytes 262176 | tf_op jit(solution)/shard_map/ppermute | solution.py:255
  42.2 2.5 %collective-permute-start.4 = (bf16[512,128]{1,0:T(8,128)(2,1)S(1)}, bf16[512,128]{1,0:T(8,128)(2,1)S(1)}, u32[]{:S(2)}, u32[]{:S(2)}) collective-permute-start(bf16[512,128]{1,0:T(8,128)(2,1)S(1)} %bitcast.38), channel_id=1, source_target_pairs={{0,16},{16,0},{1,17},{17,1},{2,18},{18,2},{3,19},{19,3},{4,20},{20... | collective-permute-start | bytes 393224 | tf_op jit(solution)/shard_map/ppermute | solution.py:270
  46.5 56.9 %all_to_all.25.x_ref = bf16[16,1024,128]{2,1,0:T(8,128)(2,1)S(1)} all-to-all(bf16[16,1024,128]{2,1,0:T(8,128)(2,1)S(1)} %broadcast_in_dim.2), channel_id=1, replica_groups=mesh['z'=16,'c'=2,'tp'=16] {'tp'}, dimensions={0} | all-to-all | bytes 8388608 | tf_op jit(solution)/shard_map/all_to_all | solution.py:272
  103.4 4.9 %shard_map.123 = bf16[16,1024,128]{2,1,0:T(8,128)(2,1)S(1)} custom-call(s32[1]{0:T(128)} %bitcast.me_ref, bf16[16,1024,128]{2,1,0:T(8,128)(2,1)S(1)} %all_to_all.25.x_ref, bf16[2048,256]{1,0:T(8,128)(2,1)S(1)} %bitcast.29, bf16[2048,256]{1,0:T(8,128)(2,1)S(1)} %bitcast.30, bf16[256,2048]{1,0:T(8,128)(2,1)S(1)} %bitcast.31), custom_call_target="tpu_custom_call" | custom-call | flops 3221225472 | bytes 11534336 | tf_op jit(solution)/shard_map/pallas_call | solution.py:91
  108.3 29.5 %all_to_all.26 = bf16[4,4,1024,128]{3,2,1,0:T(8,128)(2,1)S(1)} all-to-all(bf16[4,4,1024,128]{3,2,1,0:T(8,128)(2,1)S(1)} %bitcast.26), channel_id=1, replica_groups={{0,1,2,3},{4,5,6,7},{8,9,10,11},{12,13,14,15},{16,20,24,28},{17,21,25,2..., dimensions={0} | all-to-all | bytes 8388608 | tf_op jit(solution)/shard_map/all_to_all | solution.py:265
  137.8 3.2 %shard_map.124 = bf16[4096,128]{1,0:T(8,128)(2,1)} custom-call(bf16[4,4096,128]{2,1,0:T(8,128)(2,1)S(1)} %bitcast.25), custom_call_target="tpu_custom_call" | custom-call | tf_op jit(solution)/shard_map/pallas_call | solution.py:166
  140.9 3.6 %all-to-all-start.3 = ((bf16[4,1024,128]{2,1,0:T(8,128)(2,1)}), bf16[4,1024,128]{2,1,0:T(8,128)(2,1)S(1)}, u32[]{:S(2)}, u32[]{:S(2)}) async-start(bf16[4,1024,128]{2,1,0:T(8,128)(2,1)} %bitcast.13), calls=%async_computation.3 | async-start | bytes 2097152 | tf_op jit(solution)/shard_map/all_to_all | solution.py:265
  144.6 3.3 %collective-permute-start.7 = (bf16[8,32,2048]{2,1,0:T(8,128)(2,1)S(1)}, bf16[8,32,2048]{2,1,0:T(8,128)(2,1)S(1)}, u32[]{:S(2)}, u32[]{:S(2)}) collective-permute-start(bf16[8,32,2048]{2,1,0:T(8,128)(2,1)S(1)} %pad_maximum_fusion.y0_ref), channel_id=1, source_target_pairs={{0,4},{1,5},{2,6},{3,7},{4,8},{5,9},{6,10},{7,11},{8,12},{9,13},{1... | collective-permute-start | bytes 3145736 | tf_op jit(solution)/shard_map/ppermute | solution.py:255
  147.9 3.2 %collective-permute-start.6 = (bf16[8,32,2048]{2,1,0:T(8,128)(2,1)S(1)}, bf16[8,32,2048]{2,1,0:T(8,128)(2,1)}, u32[]{:S(2)}, u32[]{:S(2)}) collective-permute-start(bf16[8,32,2048]{2,1,0:T(8,128)(2,1)S(1)} %pad_maximum_fusion.y0_ref), channel_id=1, source_target_pairs={{0,12},{1,13},{2,14},{3,15},{4,0},{5,1},{6,2},{7,3},{8,4},{9,5},{1... | collective-permute-start | bytes 3145736 | tf_op jit(solution)/shard_map/ppermute | solution.py:255
  151.1 3.3 %all-to-all-done.3.in_ref = bf16[4,1024,128]{2,1,0:T(8,128)(2,1)S(1)} async-done(((bf16[4,1024,128]{2,1,0:T(8,128)(2,1)}), bf16[4,1024,128]{2,1,0:T(8,128)(2,1)S(1)}, u32[]{:S(2)}, u32[]{:S(2)}) %all-to-all-start.3) | async-done | bytes 1048608 | tf_op jit(solution)/shard_map/all_to_all | solution.py:265
  154.7 5.7 %collective-permute-start.5 = (bf16[512,128]{1,0:T(8,128)(2,1)S(1)}, bf16[512,128]{1,0:T(8,128)(2,1)S(1)}, u32[]{:S(2)}, u32[]{:S(2)}) collective-permute-start(bf16[512,128]{1,0:T(8,128)(2,1)S(1)} %get-tuple-element.25), channel_id=1, source_target_pairs={{0,16},{16,0},{1,17},{17,1},{2,18},{18,2},{3,19},{19,3},{4,20},{20... | collective-permute-start | bytes 393224 | tf_op jit(solution)/shard_map/ppermute | solution.py:286
  162.0 9.8 %all-to-all-start.4 = ((bf16[16,2,32,128]{3,2,1,0:T(8,128)(2,1)}), bf16[16,2,32,128]{3,2,1,0:T(8,128)(2,1)S(1)}, u32[]{:S(2)}, u32[]{:S(2)}) async-start(bf16[16,2,32,128]{3,2,1,0:T(8,128)(2,1)} %pad_maximum_fusion.2), calls=%async_computation.4 | async-start | bytes 524288 | tf_op jit(solution)/shard_map/all_to_all | solution.py:296
  172.7 2.2 %collective-permute-start.8 = (bf16[4,32,2048]{2,1,0:T(8,128)(2,1)}, bf16[4,32,2048]{2,1,0:T(8,128)(2,1)S(1)}, u32[]{:S(2)}, u32[]{:S(2)}) collective-permute-start(bf16[4,32,2048]{2,1,0:T(8,128)(2,1)} %slice.58), channel_id=1, source_target_pairs={{0,4},{1,5},{2,6},{3,7},{4,8},{5,9},{6,10},{7,11},{8,12},{9,13},{1... | collective-permute-start | bytes 1572872 | tf_op jit(solution)/shard_map/ppermute | solution.py:255
  174.9 1.9 slice.59
  176.8 4.3 %collective-permute-start.9 = (bf16[4,32,2048]{2,1,0:T(8,128)(2,1)}, bf16[4,32,2048]{2,1,0:T(8,128)(2,1)}, u32[]{:S(2)}, u32[]{:S(2)}) collective-permute-start(bf16[4,32,2048]{2,1,0:T(8,128)(2,1)} %slice.59), channel_id=1, source_target_pairs={{0,12},{1,13},{2,14},{3,15},{4,0},{5,1},{6,2},{7,3},{8,4},{9,5},{1... | collective-permute-start | bytes 1572872 | tf_op jit(solution)/shard_map/ppermute | solution.py:255
  181.9 2.4 %collective-permute-done.8.y2a_ref = bf16[4,32,2048]{2,1,0:T(8,128)(2,1)S(1)} collective-permute-done((bf16[4,32,2048]{2,1,0:T(8,128)(2,1)}, bf16[4,32,2048]{2,1,0:T(8,128)(2,1)S(1)}, u32[]{:S(2)}, u32[]{:S(2)}) %collective-permute-start.8) | collective-permute-done | bytes 524320 | tf_op jit(solution)/shard_map/ppermute | solution.py:255
  184.3 3.2 %collective-permute-done.9.y2b_ref = bf16[4,32,2048]{2,1,0:T(8,128)(2,1)} collective-permute-done((bf16[4,32,2048]{2,1,0:T(8,128)(2,1)}, bf16[4,32,2048]{2,1,0:T(8,128)(2,1)}, u32[]{:S(2)}, u32[]{:S(2)}) %collective-permute-start.9) | collective-permute-done | bytes 524320 | tf_op jit(solution)/shard_map/ppermute | solution.py:255
  187.5 4.2 %shard_map.126 = bf16[2048,128]{1,0:T(8,128)(2,1)} custom-call(s32[1]{0:T(128)} %bitcast.me_ref, bf16[8,32,2048]{2,1,0:T(8,128)(2,1)S(1)} %pad_maximum_fusion.y0_ref, bf16[8,32,2048]{2,1,0:T(8,128)(2,1)} %collective-permute-done.6.y1_ref, bf16[4,32,2048]{2,1,0:T(8,128)(2,1)S(1)} %collective-permute-done.8.y2a_ref, ...), custom_call_target="tpu_custom_call" | custom-call | flops 536870912 | bytes 4980736 | tf_op jit(solution)/shard_map/pallas_call | solution.py:143
  (38 shorter events, 12.6 us)
Async XLA Ops:
  0.6 23.4 %copy-start = (f32[3,1024]{1,0:T(4,128)S(1)}, f32[3,1024]{1,0:T(4,128)}, u32[]{:S(2)}) copy-start(f32[3,1024]{1,0:T(4,128)} %param.14) | copy-start | bytes 36868
  1.5 0.8 copy-start.2
  5.1 19.1 %collective-permute-start = (bf16[64,2]{1,0:T(8,128)(2,1)S(1)}, bf16[64,2]{1,0:T(8,128)(2,1)S(1)}, u32[]{:S(2)}, u32[]{:S(2)}) collective-permute-start(bf16[64,2]{1,0:T(8,128)(2,1)S(1)} %slice.52), channel_id=1, source_target_pairs={{0,16},{16,32},{32,48},{48,64},{64,80},{80,96},{96,112},{112,128},... | collective-permute-start | bytes 776 | tf_op jit(solution)/shard_map/ppermute | solution.py:229
  10.0 32.1 %all-to-all-start = ((bf16[16,2,32,128]{3,2,1,0:T(8,128)(2,1)}), bf16[16,2,32,128]{3,2,1,0:T(8,128)(2,1)S(1)}, u32[]{:S(2)}, u32[]{:S(2)}) async-start(bf16[16,2,32,128]{3,2,1,0:T(8,128)(2,1)} %bitcast.1), calls=%async_computation | async-start | bytes 524288 | tf_op jit(solution)/shard_map/all_to_all | solution.py:219
  25.6 9.5 %collective-permute-start.1 = (bf16[2,32,2048]{2,1,0:T(8,128)(2,1)S(1)}, bf16[2,32,2048]{2,1,0:T(8,128)(2,1)S(1)}, u32[]{:S(2)}, u32[]{:S(2)}) collective-permute-start(bf16[2,32,2048]{2,1,0:T(8,128)(2,1)S(1)} %bitcast.32), channel_id=1, source_target_pairs={{0,3},{1,0},{2,1},{3,2},{4,7},{5,4},{6,5},{7,6},{8,11},{9,8},{10,9... | collective-permute-start | bytes 786440 | tf_op jit(solution)/shard_map/ppermute | solution.py:255
  30.3 8.9 %collective-permute-start.2 = (bf16[2,32,2048]{2,1,0:T(8,128)(2,1)S(1)}, bf16[2,32,2048]{2,1,0:T(8,128)(2,1)S(1)}, u32[]{:S(2)}, u32[]{:S(2)}) collective-permute-start(bf16[2,32,2048]{2,1,0:T(8,128)(2,1)S(1)} %bitcast.33), channel_id=1, source_target_pairs={{0,2},{1,3},{2,0},{3,1},{4,6},{5,7},{6,4},{7,5},{8,10},{9,11},{10,... | collective-permute-start | bytes 786440 | tf_op jit(solution)/shard_map/ppermute | solution.py:255
  32.5 9.5 %collective-permute-start.3 = (bf16[2,32,2048]{2,1,0:T(8,128)(2,1)S(1)}, bf16[2,32,2048]{2,1,0:T(8,128)(2,1)S(1)}, u32[]{:S(2)}, u32[]{:S(2)}) collective-permute-start(bf16[2,32,2048]{2,1,0:T(8,128)(2,1)S(1)} %bitcast.34), channel_id=1, source_target_pairs={{0,1},{1,2},{2,3},{3,0},{4,5},{5,6},{6,7},{7,4},{8,9},{9,10},{10,1... | collective-permute-start | bytes 786440 | tf_op jit(solution)/shard_map/ppermute | solution.py:255
  42.2 3.5 %collective-permute-start.4 = (bf16[512,128]{1,0:T(8,128)(2,1)S(1)}, bf16[512,128]{1,0:T(8,128)(2,1)S(1)}, u32[]{:S(2)}, u32[]{:S(2)}) collective-permute-start(bf16[512,128]{1,0:T(8,128)(2,1)S(1)} %bitcast.38), channel_id=1, source_target_pairs={{0,16},{16,0},{1,17},{17,1},{2,18},{18,2},{3,19},{19,3},{4,20},{20... | collective-permute-start | bytes 393224 | tf_op jit(solution)/shard_map/ppermute | solution.py:270
  46.5 56.9 %copy-start.3 = (bf16[1,2048,256]{2,1,0:T(8,128)(2,1)S(1)}, bf16[1,2048,256]{2,1,0:T(8,128)(2,1)}, u32[]{:S(2)}) copy-start(bf16[1,2048,256]{2,1,0:T(8,128)(2,1)} %param.19) | copy-start | bytes 3145732
  46.5 56.9 %copy-start.4 = (bf16[1,2048,256]{2,1,0:T(8,128)(2,1)S(1)}, bf16[1,2048,256]{2,1,0:T(8,128)(2,1)}, u32[]{:S(2)}) copy-start(bf16[1,2048,256]{2,1,0:T(8,128)(2,1)} %param.20) | copy-start | bytes 3145732
  46.5 56.9 %copy-start.5 = (bf16[1,256,2048]{2,1,0:T(8,128)(2,1)S(1)}, bf16[1,256,2048]{2,1,0:T(8,128)(2,1)}, u32[]{:S(2)}) copy-start(bf16[1,256,2048]{2,1,0:T(8,128)(2,1)} %param.21) | copy-start | bytes 3145732
  140.9 46.6 %copy-start.1 = (bf16[1024,128]{1,0:T(8,128)(2,1)S(1)}, bf16[1024,128]{1,0:T(8,128)(2,1)}, u32[]{:S(2)}) copy-start(bf16[1024,128]{1,0:T(8,128)(2,1)} %param.15) | copy-start | bytes 786436
  140.9 13.5 %all-to-all-start.3 = ((bf16[4,1024,128]{2,1,0:T(8,128)(2,1)}), bf16[4,1024,128]{2,1,0:T(8,128)(2,1)S(1)}, u32[]{:S(2)}, u32[]{:S(2)}) async-start(bf16[4,1024,128]{2,1,0:T(8,128)(2,1)} %bitcast.13), calls=%async_computation.3 | async-start | bytes 2097152 | tf_op jit(solution)/shard_map/all_to_all | solution.py:265
  144.6 27.3 %collective-permute-start.7 = (bf16[8,32,2048]{2,1,0:T(8,128)(2,1)S(1)}, bf16[8,32,2048]{2,1,0:T(8,128)(2,1)S(1)}, u32[]{:S(2)}, u32[]{:S(2)}) collective-permute-start(bf16[8,32,2048]{2,1,0:T(8,128)(2,1)S(1)} %pad_maximum_fusion.y0_ref), channel_id=1, source_target_pairs={{0,4},{1,5},{2,6},{3,7},{4,8},{5,9},{6,10},{7,11},{8,12},{9,13},{1... | collective-permute-start | bytes 3145736 | tf_op jit(solution)/shard_map/ppermute | solution.py:255
  147.9 27.0 %collective-permute-start.6 = (bf16[8,32,2048]{2,1,0:T(8,128)(2,1)S(1)}, bf16[8,32,2048]{2,1,0:T(8,128)(2,1)}, u32[]{:S(2)}, u32[]{:S(2)}) collective-permute-start(bf16[8,32,2048]{2,1,0:T(8,128)(2,1)S(1)} %pad_maximum_fusion.y0_ref), channel_id=1, source_target_pairs={{0,12},{1,13},{2,14},{3,15},{4,0},{5,1},{6,2},{7,3},{8,4},{9,5},{1... | collective-permute-start | bytes 3145736 | tf_op jit(solution)/shard_map/ppermute | solution.py:255
  154.7 6.6 %collective-permute-start.5 = (bf16[512,128]{1,0:T(8,128)(2,1)S(1)}, bf16[512,128]{1,0:T(8,128)(2,1)S(1)}, u32[]{:S(2)}, u32[]{:S(2)}) collective-permute-start(bf16[512,128]{1,0:T(8,128)(2,1)S(1)} %get-tuple-element.25), channel_id=1, source_target_pairs={{0,16},{16,0},{1,17},{17,1},{2,18},{18,2},{3,19},{19,3},{4,20},{20... | collective-permute-start | bytes 393224 | tf_op jit(solution)/shard_map/ppermute | solution.py:286
  162.0 29.7 %all-to-all-start.4 = ((bf16[16,2,32,128]{3,2,1,0:T(8,128)(2,1)}), bf16[16,2,32,128]{3,2,1,0:T(8,128)(2,1)S(1)}, u32[]{:S(2)}, u32[]{:S(2)}) async-start(bf16[16,2,32,128]{3,2,1,0:T(8,128)(2,1)} %pad_maximum_fusion.2), calls=%async_computation.4 | async-start | bytes 524288 | tf_op jit(solution)/shard_map/all_to_all | solution.py:296
  172.7 11.6 %collective-permute-start.8 = (bf16[4,32,2048]{2,1,0:T(8,128)(2,1)}, bf16[4,32,2048]{2,1,0:T(8,128)(2,1)S(1)}, u32[]{:S(2)}, u32[]{:S(2)}) collective-permute-start(bf16[4,32,2048]{2,1,0:T(8,128)(2,1)} %slice.58), channel_id=1, source_target_pairs={{0,4},{1,5},{2,6},{3,7},{4,8},{5,9},{6,10},{7,11},{8,12},{9,13},{1... | collective-permute-start | bytes 1572872 | tf_op jit(solution)/shard_map/ppermute | solution.py:255
  176.8 10.7 %collective-permute-start.9 = (bf16[4,32,2048]{2,1,0:T(8,128)(2,1)}, bf16[4,32,2048]{2,1,0:T(8,128)(2,1)}, u32[]{:S(2)}, u32[]{:S(2)}) collective-permute-start(bf16[4,32,2048]{2,1,0:T(8,128)(2,1)} %slice.59), channel_id=1, source_target_pairs={{0,12},{1,13},{2,14},{3,15},{4,0},{5,1},{6,2},{7,3},{8,4},{9,5},{1... | collective-permute-start | bytes 1572872 | tf_op jit(solution)/shard_map/ppermute | solution.py:255

commit v2 on v1

--- a/solution.py
+++ b/solution.py
@@ -65,18 +65,36 @@
     out_ref[...] = total.astype(BF)
 
 
-def expert_kernel(me_ref, x_ref, gate_ref, up_ref, down_ref, out_ref):
+def expert_kernel(me_ref, x_ref, *refs):
+    sources, (out_ref, gate_ref, up_ref, down_ref, sems) = refs[:3], refs[3:]
+    copies = [
+        pltpu.make_async_copy(source, target, sems.at[k])
+        for k, (source, target) in enumerate(zip(sources, (gate_ref, up_ref, down_ref)))
+    ]
+
+    @pl.when(pl.program_id(0) == 0)
+    def _():
+        for copy in copies:
+            copy.start()
+
     parts = x_ref.shape[0]
     cols = x_ref.shape[2]
     side = 4
     core = me_ref[0] // parts
     natural = [j for j in range(parts)]
     turned = [(j % side) * side + j // side for j in range(parts)]
+    load = [jnp.where(core == 0, natural[j], turned[j]) for j in range(parts)]
     store = [jnp.where(core == 0, turned[j], natural[j]) for j in range(parts)]
-    x = jnp.concatenate([x_ref[j] for j in range(parts)], axis=1)
+    x = jnp.concatenate([x_ref[load[j]] for j in range(parts)], axis=1)
     values = x.astype(F32)
     squares = jnp.sum(values * values, axis=1, keepdims=True)
     scale = lax.rsqrt(squares / (parts * cols) + EPSILON)
+
+    @pl.when(pl.program_id(0) == 0)
+    def _():
+        for copy in copies:
+            copy.wait()
+
     gate = scale * jnp.dot(x, gate_ref[...], preferred_element_type=F32)
     up = scale * jnp.dot(x, up_ref[...], preferred_element_type=F32)
     hidden = (jax.nn.silu(gate) * up).astype(BF)
@@ -87,7 +105,7 @@
 
 def expert_part(me, x, gate_weight, up_weight, down_weight, tile):
     parts, rows, cols = x.shape
-    whole = lambda w: pl.BlockSpec(w.shape, lambda i, c: (0, 0))
+    stays = pl.BlockSpec(memory_space=pltpu.HBM)
     return pl.pallas_call(
         expert_kernel,
         grid_spec=pltpu.PrefetchScalarGridSpec(
@@ -95,11 +113,17 @@
             grid=(rows // tile,),
             in_specs=[
                 pl.BlockSpec((parts, tile, cols), lambda i, c: (0, i, 0)),
-                whole(gate_weight),
-                whole(up_weight),
-                whole(down_weight),
+                stays,
+                stays,
+                stays,
             ],
             out_specs=pl.BlockSpec((parts, tile, cols), lambda i, c: (0, i, 0)),
+            scratch_shapes=[
+                pltpu.VMEM(gate_weight.shape, BF),
+                pltpu.VMEM(up_weight.shape, BF),
+                pltpu.VMEM(down_weight.shape, BF),
+                pltpu.SemaphoreType.DMA((3,)),
+            ],
         ),
         out_shape=jax.ShapeDtypeStruct(x.shape, BF),
         compiler_params=pltpu.CompilerParams(vmem_limit_bytes=28 * 1024 * 1024),
@@ -269,19 +293,29 @@
     rows_own = arrived[:, 0].reshape(half, cols_part)
     rows_other = lax.ppermute(arrived[:, 1].reshape(half, cols_part), "c", swap)
     rows = jnp.concatenate([rows_own, rows_other], axis=0)
-    x = lax.all_to_all(
-        jnp.broadcast_to(rows[None], (tp,) + rows.shape), "tp", 0, 0, tiled=True
-    )
+    quarter = exchange(jnp.broadcast_to(rows[None], (side,) + rows.shape), early)
+    line_before = step(line, 1, 1)
+    line_after = step(line, -1, 1)
+    quarter, line_before, line_after = lax.optimization_barrier(
+        (quarter, line_before, line_after)
+    )
+    x = exchange(jnp.broadcast_to(quarter[None], (side,) + quarter.shape), late)
+    line_far_a = step(line_before[:4], 1, 1)
+    line_far_b = step(line_after[4:], -1, 1)
+    mixed_out = mixer_product(
+        me,
+        (line, line_after, line_far_a, line_far_b, line_before),
+        mixer_proj.reshape(tp, width_part, cols_part),
+        length // 4,
+    )
+    x, mixed_out = lax.optimization_barrier((x, mixed_out))
+    x = x.reshape(tp, slot_total, cols_part)
     weights = (expert_gate[0], expert_up[0], expert_down[0])
     part = expert_part(me, x, *weights, rows_b)
     part = part.reshape(side, side, slot_total, cols_part)
     half_sums = exchange(part, early).reshape(side, side * slot_total, cols_part)
     half_sums = sum_parts(half_sums, 8).reshape(side, slot_total, cols_part)
-    half_sums, line = lax.optimization_barrier((half_sums, line))
-    line_before = step(line, 1, 1)
-    line_after = step(line, -1, 1)
-    expert_rows = exchange(half_sums, late)
-    expert_rows = sum_parts(expert_rows, 2)
+    expert_rows = sum_parts(exchange(half_sums, late), 2)
     back_own = expert_rows[:half]
     back_other = lax.ppermute(expert_rows[half:], "c", swap)
     back = jnp.stack(
@@ -291,16 +325,7 @@
         ],
         axis=1,
     )
-    line_far_a = step(line_before[:4], 1, 1)
-    line_far_b = step(line_after[4:], -1, 1)
     returned = lax.all_to_all(back, "z", 0, 0, tiled=True)
-    mixed_out = mixer_product(
-        me,
-        (line, line_after, line_far_a, line_far_b, line_before),
-        mixer_proj.reshape(tp, width_part, cols_part),
-        length // 4,
-    )
-    returned, mixed_out = lax.optimization_barrier((returned, mixed_out))
     returned = returned.reshape(slot_total, cols_part)
     expert_out = pl.pallas_call(
         combine_kernel,

time: 195 us -> 203 us (1.041)
  the two profiles are of different devices: /device:TPU:1 before, /device:TPU:32 now
where the time goes in v2:
time: 203 us; the launch traced here: 201 us
  starting transfers between devices  61.1 us (30%)
  blocking collectives  59.8 us (29%)
  waiting for transfers between devices  53.8 us (27%)
  Pallas kernels  13.7 us (7%)
  local copies, waits for them, and re-layouts  8.72 us (4%)
  other arithmetic  3.43 us (2%)
    all_to_all x3, blocking collectives, exchange(): lax.all_to_all(value, ('c', 'tp'), 0, 0, axis_index_groups=groups, tiled=...  59.8 us
    ppermute x7, waiting for transfers between devices, step(): return lax.ppermute(value, ('c', 'tp'), pairs)  32.9 us
    ppermute x7, starting transfers between devices, step(): return lax.ppermute(value, ('c', 'tp'), pairs)  24.4 us
    all_to_all x1, waiting for transfers between devices, layer(): returned = lax.all_to_all(back, 'z', 0, 0, tiled=True)  18.2 us
    all_to_all x1, starting transfers between devices, layer(): lax.all_to_all(outgoing.reshape(depth, 2, capacity, cols_part), 'z', 0, 0...  15.2 us
    all_to_all x1, starting transfers between devices, layer(): returned = lax.all_to_all(back, 'z', 0, 0, tiled=True)  10.7 us
    pallas_call x1, Pallas kernels, expert_part(): pl.pallas_call(expert_kernel, grid_spec=pltpu.PrefetchScalarGridSpec(num_...  6.9 us
    unnamed x16, local copies, waits for them, and re-layouts  5.47 us
  transfers between devices with their start and end apart: 13, of which 6 were waited for; matrix products, arithmetic and copies ran while one was open for 1% of the time, Pallas kernels for 1%

profile of v2, /device:TPU:32, one launch (start us, length us, event | category | flops | bytes accessed | tf_op | source)
XLA Modules:
  0.0 201.5 jit_solution(18063439010698729909)
XLA Ops:
  2.3 1.6 shard_map.122
  5.1 1.9 collective-permute-start
  7.0 15.2 %all-to-all-start = ((bf16[16,2,32,128]{3,2,1,0:T(8,128)(2,1)}), bf16[16,2,32,128]{3,2,1,0:T(8,128)(2,1)S(1)}, u32[]{:S(2)}, u32[]{:S(2)}) async-start(bf16[16,2,32,128]{3,2,1,0:T(8,128)(2,1)} %bitcast.1), calls=%async_computation | async-start | bytes 524288 | tf_op jit(solution)/shard_map/all_to_all | solution.py:243
  23.8 4.7 %collective-permute-start.1 = (bf16[2,32,2048]{2,1,0:T(8,128)(2,1)S(1)}, bf16[2,32,2048]{2,1,0:T(8,128)(2,1)S(1)}, u32[]{:S(2)}, u32[]{:S(2)}) collective-permute-start(bf16[2,32,2048]{2,1,0:T(8,128)(2,1)S(1)} %bitcast.34), channel_id=1, source_target_pairs={{0,3},{1,0},{2,1},{3,2},{4,7},{5,4},{6,5},{7,6},{8,11},{9,8},{10,9... | collective-permute-start | bytes 786440 | tf_op jit(solution)/shard_map/ppermute | solution.py:279
  28.5 2.7 %collective-permute-start.2 = (bf16[2,32,2048]{2,1,0:T(8,128)(2,1)S(1)}, bf16[2,32,2048]{2,1,0:T(8,128)(2,1)S(1)}, u32[]{:S(2)}, u32[]{:S(2)}) collective-permute-start(bf16[2,32,2048]{2,1,0:T(8,128)(2,1)S(1)} %bitcast.35), channel_id=1, source_target_pairs={{0,2},{1,3},{2,0},{3,1},{4,6},{5,7},{6,4},{7,5},{8,10},{9,11},{10,... | collective-permute-start | bytes 786440 | tf_op jit(solution)/shard_map/ppermute | solution.py:279
  31.2 2.8 %collective-permute-start.3 = (bf16[2,32,2048]{2,1,0:T(8,128)(2,1)S(1)}, bf16[2,32,2048]{2,1,0:T(8,128)(2,1)S(1)}, u32[]{:S(2)}, u32[]{:S(2)}) collective-permute-start(bf16[2,32,2048]{2,1,0:T(8,128)(2,1)S(1)} %bitcast.36), channel_id=1, source_target_pairs={{0,1},{1,2},{2,3},{3,0},{4,5},{5,6},{6,7},{7,4},{8,9},{9,10},{10,1... | collective-permute-start | bytes 786440 | tf_op jit(solution)/shard_map/ppermute | solution.py:279
  34.0 4.3 %collective-permute-done.2 = bf16[2,32,2048]{2,1,0:T(8,128)(2,1)S(1)} collective-permute-done((bf16[2,32,2048]{2,1,0:T(8,128)(2,1)S(1)}, bf16[2,32,2048]{2,1,0:T(8,128)(2,1)S(1)}, u32[]{:S(2)}, u32[]{:S(2)}) %collective-permute-start.2) | collective-permute-done | bytes 262176 | tf_op jit(solution)/shard_map/ppermute | solution.py:279
  38.3 2.8 %collective-permute-done.3 = bf16[2,32,2048]{2,1,0:T(8,128)(2,1)S(1)} collective-permute-done((bf16[2,32,2048]{2,1,0:T(8,128)(2,1)S(1)}, bf16[2,32,2048]{2,1,0:T(8,128)(2,1)S(1)}, u32[]{:S(2)}, u32[]{:S(2)}) %collective-permute-start.3) | collective-permute-done | bytes 262176 | tf_op jit(solution)/shard_map/ppermute | solution.py:279
  41.2 3.5 %collective-permute-start.5 = (bf16[8,32,2048]{2,1,0:T(8,128)(2,1)S(1)}, bf16[8,32,2048]{2,1,0:T(8,128)(2,1)S(1)}, u32[]{:S(2)}, u32[]{:S(2)}) collective-permute-start(bf16[8,32,2048]{2,1,0:T(8,128)(2,1)S(1)} %pad_maximum_fusion.y0_ref), channel_id=1, source_target_pairs={{0,4},{1,5},{2,6},{3,7},{4,8},{5,9},{6,10},{7,11},{8,12},{9,13},{1... | collective-permute-start | bytes 3145736 | tf_op jit(solution)/shard_map/ppermute | solution.py:279
  44.7 3.6 %collective-permute-start.6 = (bf16[8,32,2048]{2,1,0:T(8,128)(2,1)S(1)}, bf16[8,32,2048]{2,1,0:T(8,128)(2,1)S(1)}, u32[]{:S(2)}, u32[]{:S(2)}) collective-permute-start(bf16[8,32,2048]{2,1,0:T(8,128)(2,1)S(1)} %pad_maximum_fusion.y0_ref), channel_id=1, source_target_pairs={{0,12},{1,13},{2,14},{3,15},{4,0},{5,1},{6,2},{7,3},{8,4},{9,5},{1... | collective-permute-start | bytes 3145736 | tf_op jit(solution)/shard_map/ppermute | solution.py:279
  48.3 1.9 collective-permute-start.4
  51.7 14.7 %all_to_all.30 = bf16[4,1024,128]{2,1,0:T(8,128)(2,1)S(1)} all-to-all(bf16[4,1024,128]{2,1,0:T(8,128)(2,1)S(1)} %broadcast_in_dim.4), channel_id=1, replica_groups={{0,1,2,3},{4,5,6,7},{8,9,10,11},{12,13,14,15},{16,20,24,28},{17,21,25,2..., dimensions={0} | all-to-all | bytes 2097152 | tf_op jit(solution)/shard_map/all_to_all | solution.py:289
  66.4 2.8 %broadcast_in_dim.5 = bf16[4,4,1024,128]{3,2,1,0:T(8,128)(2,1)} broadcast(bf16[4,1024,128]{2,1,0:T(8,128)(2,1)S(1)} %all_to_all.30), dimensions={1,2,3} | broadcast | bytes 5242880 | tf_op jit(solution)/shard_map/broadcast_in_dim | solution.py:302
  69.3 5.0 %all-to-all-start.2 = ((bf16[4,4,1024,128]{3,2,1,0:T(8,128)(2,1)}), bf16[4,4,1024,128]{3,2,1,0:T(8,128)(2,1)}, u32[]{:S(2)}, u32[]{:S(2)}) async-start(bf16[4,4,1024,128]{3,2,1,0:T(8,128)(2,1)} %broadcast_in_dim.5), calls=%async_computation.2 | async-start | bytes 8388608 | tf_op jit(solution)/shard_map/all_to_all | solution.py:289
  74.3 3.9 %collective-permute-start.7 = (bf16[4,32,2048]{2,1,0:T(8,128)(2,1)S(1)}, bf16[4,32,2048]{2,1,0:T(8,128)(2,1)S(1)}, u32[]{:S(2)}, u32[]{:S(2)}) collective-permute-start(bf16[4,32,2048]{2,1,0:T(8,128)(2,1)S(1)} %slice.48), channel_id=1, source_target_pairs={{0,4},{1,5},{2,6},{3,7},{4,8},{5,9},{6,10},{7,11},{8,12},{9,13},{1... | collective-permute-start | bytes 1572872 | tf_op jit(solution)/shard_map/ppermute | solution.py:279
  78.3 3.3 %collective-permute-start.8 = (bf16[4,32,2048]{2,1,0:T(8,128)(2,1)S(1)}, bf16[4,32,2048]{2,1,0:T(8,128)(2,1)S(1)}, u32[]{:S(2)}, u32[]{:S(2)}) collective-permute-start(bf16[4,32,2048]{2,1,0:T(8,128)(2,1)S(1)} %slice.49), channel_id=1, source_target_pairs={{0,12},{1,13},{2,14},{3,15},{4,0},{5,1},{6,2},{7,3},{8,4},{9,5},{1... | collective-permute-start | bytes 1572872 | tf_op jit(solution)/shard_map/ppermute | solution.py:279
  81.6 25.9 %collective-permute-done.7.y2a_ref = bf16[4,32,2048]{2,1,0:T(8,128)(2,1)S(1)} collective-permute-done((bf16[4,32,2048]{2,1,0:T(8,128)(2,1)S(1)}, bf16[4,32,2048]{2,1,0:T(8,128)(2,1)S(1)}, u32[]{:S(2)}, u32[]{:S(2)}) %collective-permute-start.7) | collective-permute-done | bytes 524320 | tf_op jit(solution)/shard_map/ppermute | solution.py:279
  107.5 2.9 %shard_map.123 = bf16[2048,128]{1,0:T(8,128)(2,1)} custom-call(s32[1]{0:T(128)} %bitcast.me_ref, bf16[8,32,2048]{2,1,0:T(8,128)(2,1)S(1)} %pad_maximum_fusion.y0_ref, bf16[8,32,2048]{2,1,0:T(8,128)(2,1)S(1)} %collective-permute-done.6.y1_ref, bf16[4,32,2048]{2,1,0:T(8,128)(2,1)S(1)} %collective-permute-done.7.y2a_ref, ...), custom_call_target="tpu_custom_call" | custom-call | flops 536870912 | bytes 4980736 | tf_op jit(solution)/shard_map/pallas_call | solution.py:167
  114.1 6.9 %shard_map.124 = bf16[16,1024,128]{2,1,0:T(8,128)(2,1)S(1)} custom-call(s32[1]{0:T(128)} %bitcast.me_ref, bf16[16,1024,128]{2,1,0:T(8,128)(2,1)} %bitcast.9.x_ref, bf16[2048,256]{1,0:T(8,128)(2,1)S(1)} %bitcast.31, bf16[2048,256]{1,0:T(8,128)(2,1)S(1)} %bitcast.32, bf16[256,2048]{1,0:T(8,128)(2,1)S(1)} %bitcast.33), custom_call_target="tpu_custom_call" | custom-call | flops 3221225472 | bytes 11534336 | tf_op jit(solution)/shard_map/pallas_call | solution.py:109
  121.0 31.6 %all_to_all.31 = bf16[4,4,1024,128]{3,2,1,0:T(8,128)(2,1)S(1)} all-to-all(bf16[4,4,1024,128]{3,2,1,0:T(8,128)(2,1)S(1)} %bitcast.28), channel_id=1, replica_groups={{0,1,2,3},{4,5,6,7},{8,9,10,11},{12,13,14,15},{16,20,24,28},{17,21,25,2..., dimensions={0} | all-to-all | bytes 8388608 | tf_op jit(solution)/shard_map/all_to_all | solution.py:289
  153.5 13.5 %all_to_all.32.in_ref = bf16[4,1024,128]{2,1,0:T(8,128)(2,1)S(1)} all-to-all(bf16[4,1024,128]{2,1,0:T(8,128)(2,1)S(1)} %bitcast.27), channel_id=1, replica_groups={{0,4,8,12},{1,5,9,13},{2,6,10,14},{3,7,11,15},{16,17,18,19},{20,21,22,2..., dimensions={0} | all-to-all | bytes 2097152 | tf_op jit(solution)/shard_map/all_to_all | solution.py:289
  167.3 1.9 collective-permute-start.9
  171.3 10.7 %all-to-all-start.5 = ((bf16[16,2,32,128]{3,2,1,0:T(8,128)(2,1)}), bf16[16,2,32,128]{3,2,1,0:T(8,128)(2,1)S(1)}, u32[]{:S(2)}, u32[]{:S(2)}) async-start(bf16[16,2,32,128]{3,2,1,0:T(8,128)(2,1)} %pad_maximum_fusion.2), calls=%async_computation.5 | async-start | bytes 524288 | tf_op jit(solution)/shard_map/all_to_all | solution.py:328
  182.2 18.2 %all-to-all-done.5 = bf16[16,2,32,128]{3,2,1,0:T(8,128)(2,1)S(1)} async-done(((bf16[16,2,32,128]{3,2,1,0:T(8,128)(2,1)}), bf16[16,2,32,128]{3,2,1,0:T(8,128)(2,1)S(1)}, u32[]{:S(2)}, u32[]{:S(2)}) %all-to-all-start.5) | async-done | bytes 262176 | tf_op jit(solution)/shard_map/all_to_all | solution.py:328
  (42 shorter events, 14.3 us)
Async XLA Ops:
  0.6 21.6 %copy-start = (f32[3,1024]{1,0:T(4,128)S(1)}, f32[3,1024]{1,0:T(4,128)}, u32[]{:S(2)}) copy-start(f32[3,1024]{1,0:T(4,128)} %param.14) | copy-start | bytes 36868
  1.5 0.8 copy-start.2
  5.1 17.2 %collective-permute-start = (bf16[64,2]{1,0:T(8,128)(2,1)S(1)}, bf16[64,2]{1,0:T(8,128)(2,1)S(1)}, u32[]{:S(2)}, u32[]{:S(2)}) collective-permute-start(bf16[64,2]{1,0:T(8,128)(2,1)S(1)} %slice.52), channel_id=1, source_target_pairs={{0,16},{16,32},{32,48},{48,64},{64,80},{80,96},{96,112},{112,128},... | collective-permute-start | bytes 776 | tf_op jit(solution)/shard_map/ppermute | solution.py:253
  7.0 34.2 %all-to-all-start = ((bf16[16,2,32,128]{3,2,1,0:T(8,128)(2,1)}), bf16[16,2,32,128]{3,2,1,0:T(8,128)(2,1)S(1)}, u32[]{:S(2)}, u32[]{:S(2)}) async-start(bf16[16,2,32,128]{3,2,1,0:T(8,128)(2,1)} %bitcast.1), calls=%async_computation | async-start | bytes 524288 | tf_op jit(solution)/shard_map/all_to_all | solution.py:243
  23.8 10.2 %collective-permute-start.1 = (bf16[2,32,2048]{2,1,0:T(8,128)(2,1)S(1)}, bf16[2,32,2048]{2,1,0:T(8,128)(2,1)S(1)}, u32[]{:S(2)}, u32[]{:S(2)}) collective-permute-start(bf16[2,32,2048]{2,1,0:T(8,128)(2,1)S(1)} %bitcast.34), channel_id=1, source_target_pairs={{0,3},{1,0},{2,1},{3,2},{4,7},{5,4},{6,5},{7,6},{8,11},{9,8},{10,9... | collective-permute-start | bytes 786440 | tf_op jit(solution)/shard_map/ppermute | solution.py:279
  28.5 9.8 %collective-permute-start.2 = (bf16[2,32,2048]{2,1,0:T(8,128)(2,1)S(1)}, bf16[2,32,2048]{2,1,0:T(8,128)(2,1)S(1)}, u32[]{:S(2)}, u32[]{:S(2)}) collective-permute-start(bf16[2,32,2048]{2,1,0:T(8,128)(2,1)S(1)} %bitcast.35), channel_id=1, source_target_pairs={{0,2},{1,3},{2,0},{3,1},{4,6},{5,7},{6,4},{7,5},{8,10},{9,11},{10,... | collective-permute-start | bytes 786440 | tf_op jit(solution)/shard_map/ppermute | solution.py:279
  31.2 9.9 %collective-permute-start.3 = (bf16[2,32,2048]{2,1,0:T(8,128)(2,1)S(1)}, bf16[2,32,2048]{2,1,0:T(8,128)(2,1)S(1)}, u32[]{:S(2)}, u32[]{:S(2)}) collective-permute-start(bf16[2,32,2048]{2,1,0:T(8,128)(2,1)S(1)} %bitcast.36), channel_id=1, source_target_pairs={{0,1},{1,2},{2,3},{3,0},{4,5},{5,6},{6,7},{7,4},{8,9},{9,10},{10,1... | collective-permute-start | bytes 786440 | tf_op jit(solution)/shard_map/ppermute | solution.py:279
  41.2 25.2 %collective-permute-start.5 = (bf16[8,32,2048]{2,1,0:T(8,128)(2,1)S(1)}, bf16[8,32,2048]{2,1,0:T(8,128)(2,1)S(1)}, u32[]{:S(2)}, u32[]{:S(2)}) collective-permute-start(bf16[8,32,2048]{2,1,0:T(8,128)(2,1)S(1)} %pad_maximum_fusion.y0_ref), channel_id=1, source_target_pairs={{0,4},{1,5},{2,6},{3,7},{4,8},{5,9},{6,10},{7,11},{8,12},{9,13},{1... | collective-permute-start | bytes 3145736 | tf_op jit(solution)/shard_map/ppermute | solution.py:279
  44.7 21.8 %collective-permute-start.6 = (bf16[8,32,2048]{2,1,0:T(8,128)(2,1)S(1)}, bf16[8,32,2048]{2,1,0:T(8,128)(2,1)S(1)}, u32[]{:S(2)}, u32[]{:S(2)}) collective-permute-start(bf16[8,32,2048]{2,1,0:T(8,128)(2,1)S(1)} %pad_maximum_fusion.y0_ref), channel_id=1, source_target_pairs={{0,12},{1,13},{2,14},{3,15},{4,0},{5,1},{6,2},{7,3},{8,4},{9,5},{1... | collective-permute-start | bytes 3145736 | tf_op jit(solution)/shard_map/ppermute | solution.py:279
  48.3 3.2 %collective-permute-start.4 = (bf16[512,128]{1,0:T(8,128)(2,1)S(1)}, bf16[512,128]{1,0:T(8,128)(2,1)S(1)}, u32[]{:S(2)}, u32[]{:S(2)}) collective-permute-start(bf16[512,128]{1,0:T(8,128)(2,1)S(1)} %bitcast.40), channel_id=1, source_target_pairs={{0,16},{16,0},{1,17},{17,1},{2,18},{18,2},{3,19},{19,3},{4,20},{20... | collective-permute-start | bytes 393224 | tf_op jit(solution)/shard_map/ppermute | solution.py:294
  69.3 38.2 %copy-start.1 = (bf16[1024,128]{1,0:T(8,128)(2,1)S(1)}, bf16[1024,128]{1,0:T(8,128)(2,1)}, u32[]{:S(2)}) copy-start(bf16[1024,128]{1,0:T(8,128)(2,1)} %param.15) | copy-start | bytes 786436
  69.3 41.1 %all-to-all-start.2 = ((bf16[4,4,1024,128]{3,2,1,0:T(8,128)(2,1)}), bf16[4,4,1024,128]{3,2,1,0:T(8,128)(2,1)}, u32[]{:S(2)}, u32[]{:S(2)}) async-start(bf16[4,4,1024,128]{3,2,1,0:T(8,128)(2,1)} %broadcast_in_dim.5), calls=%async_computation.2 | async-start | bytes 8388608 | tf_op jit(solution)/shard_map/all_to_all | solution.py:289
  74.3 33.1 %collective-permute-start.7 = (bf16[4,32,2048]{2,1,0:T(8,128)(2,1)S(1)}, bf16[4,32,2048]{2,1,0:T(8,128)(2,1)S(1)}, u32[]{:S(2)}, u32[]{:S(2)}) collective-permute-start(bf16[4,32,2048]{2,1,0:T(8,128)(2,1)S(1)} %slice.48), channel_id=1, source_target_pairs={{0,4},{1,5},{2,6},{3,7},{4,8},{5,9},{6,10},{7,11},{8,12},{9,13},{1... | collective-permute-start | bytes 1572872 | tf_op jit(solution)/shard_map/ppermute | solution.py:279
  78.3 29.2 %collective-permute-start.8 = (bf16[4,32,2048]{2,1,0:T(8,128)(2,1)S(1)}, bf16[4,32,2048]{2,1,0:T(8,128)(2,1)S(1)}, u32[]{:S(2)}, u32[]{:S(2)}) collective-permute-start(bf16[4,32,2048]{2,1,0:T(8,128)(2,1)S(1)} %slice.49), channel_id=1, source_target_pairs={{0,12},{1,13},{2,14},{3,15},{4,0},{5,1},{6,2},{7,3},{8,4},{9,5},{1... | collective-permute-start | bytes 1572872 | tf_op jit(solution)/shard_map/ppermute | solution.py:279
  110.4 1.2 copy-start.3
  111.6 1.2 copy-start.4
  112.8 1.2 copy-start.5
  152.6 29.4 %copy-start.6 = (f32[256,2]{0,1:T(2,128)S(1)}, f32[256,2]{0,1:T(2,128)}, u32[]{:S(2)}) copy-start(f32[256,2]{0,1:T(2,128)} %param.18) | copy-start | bytes 6148
  167.3 3.2 %collective-permute-start.9 = (bf16[512,128]{1,0:T(8,128)(2,1)S(1)}, bf16[512,128]{1,0:T(8,128)(2,1)S(1)}, u32[]{:S(2)}, u32[]{:S(2)}) collective-permute-start(bf16[512,128]{1,0:T(8,128)(2,1)S(1)} %get-tuple-element.27), channel_id=1, source_target_pairs={{0,16},{16,0},{1,17},{17,1},{2,18},{18,2},{3,19},{19,3},{4,20},{20... | collective-permute-start | bytes 393224 | tf_op jit(solution)/shard_map/ppermute | solution.py:320
  171.3 29.1 %all-to-all-start.5 = ((bf16[16,2,32,128]{3,2,1,0:T(8,128)(2,1)}), bf16[16,2,32,128]{3,2,1,0:T(8,128)(2,1)S(1)}, u32[]{:S(2)}, u32[]{:S(2)}) async-start(bf16[16,2,32,128]{3,2,1,0:T(8,128)(2,1)} %pad_maximum_fusion.2), calls=%async_computation.5 | async-start | bytes 524288 | tf_op jit(solution)/shard_map/all_to_all | solution.py:328

commit v3 on v1

--- a/solution.py
+++ b/solution.py
@@ -23,36 +23,35 @@
     rows = rows_ref.shape[0]
     slot_total = out_ref.shape[0]
     capacity = slot_total // experts
-    ids = lax.broadcasted_iota(jnp.int32, (rows, experts), 1)
-    named = [routes_ref[:, k : k + 1] for k in range(2)]
+    ids = lax.broadcasted_iota(jnp.int32, (experts, rows), 0)
+    named = [routes_ref[k : k + 1, :] for k in range(2)]
     hit = [n == ids for n in named]
-    later = lax.broadcasted_iota(jnp.int32, (rows, rows), 0)
-    sooner = lax.broadcasted_iota(jnp.int32, (rows, rows), 1)
+    sooner = lax.broadcasted_iota(jnp.int32, (rows, rows), 0)
+    later = lax.broadcasted_iota(jnp.int32, (rows, rows), 1)
     earlier = jnp.dot(
-        ones_where(sooner < later), ones_where(hit[0] | hit[1]), preferred_element_type=F32
-    )
-    slots = lax.broadcasted_iota(jnp.int32, (rows, slot_total), 1)
+        ones_where(hit[0] | hit[1]), ones_where(sooner < later), preferred_element_type=F32
+    )
+    slots = lax.broadcasted_iota(jnp.int32, (slot_total, rows), 0)
     taken = []
     for k in range(2):
-        slot = jnp.sum(jnp.where(hit[k], earlier, 0.0), axis=1, keepdims=True)
+        slot = jnp.sum(jnp.where(hit[k], earlier, 0.0), axis=0, keepdims=True)
         place = (named[k] ^ core) * capacity + slot.astype(jnp.int32)
-        places_ref[:, k : k + 1] = place
+        places_ref[k : k + 1, :] = place
         taken.append(place == slots)
-    out_ref[...] = lax.dot_general(
-        ones_where(taken[0] | taken[1]),
-        rows_ref[...],
-        (((0,), (0,)), ((), ())),
-        preferred_element_type=F32,
+    out_ref[...] = jnp.dot(
+        ones_where(taken[0] | taken[1]), rows_ref[...], preferred_element_type=F32
     ).astype(BF)
 
 
 def combine_kernel(places_ref, weights_ref, returned_ref, out_ref):
     rows = out_ref.shape[0]
-    slots = lax.broadcasted_iota(jnp.int32, (rows, returned_ref.shape[0]), 1)
+    slots = lax.broadcasted_iota(jnp.int32, (returned_ref.shape[0], rows), 0)
     total = None
     for k in range(2):
-        pick = ones_where(places_ref[:, k : k + 1] == slots)
-        picked = jnp.dot(pick, returned_ref[...], preferred_element_type=F32)
+        pick = ones_where(places_ref[k : k + 1, :] == slots)
+        picked = lax.dot_general(
+            pick, returned_ref[...], (((0,), (0,)), ((), ())), preferred_element_type=F32
+        )
         term = picked * weights_ref[:, k : k + 1]
         total = term if total is None else total + term
     out_ref[...] = total.astype(BF)
@@ -72,8 +71,9 @@
     core = me_ref[0] // parts
     natural = [j for j in range(parts)]
     turned = [(j % side) * side + j // side for j in range(parts)]
+    load = [jnp.where(core == 0, natural[j], turned[j]) for j in range(parts)]
     store = [jnp.where(core == 0, turned[j], natural[j]) for j in range(parts)]
-    x = jnp.concatenate([x_ref[j] for j in range(parts)], axis=1)
+    x = jnp.concatenate([x_ref[load[j]] for j in range(parts)], axis=1)
     values = x.astype(F32)
     squares = jnp.sum(values * values, axis=1, keepdims=True)
     scale = lax.rsqrt(squares / (parts * cols) + EPSILON)
@@ -195,26 +195,27 @@
     slot_total = experts * capacity
     half = slot_total // 2
 
+    by_choice = routes.T
     places, outgoing = pl.pallas_call(
         functools.partial(dispatch_kernel, experts=experts, tp=tp),
         grid_spec=pltpu.PrefetchScalarGridSpec(
             num_scalar_prefetch=1,
             grid=(1,),
             in_specs=[
-                pl.BlockSpec(routes.shape, lambda i, c: (0, 0)),
+                pl.BlockSpec(by_choice.shape, lambda i, c: (0, 0)),
                 pl.BlockSpec(token_rows.shape, lambda i, c: (0, 0)),
             ],
             out_specs=[
-                pl.BlockSpec(routes.shape, lambda i, c: (0, 0)),
+                pl.BlockSpec(by_choice.shape, lambda i, c: (0, 0)),
                 pl.BlockSpec((slot_total, cols_part), lambda i, c: (0, 0)),
             ],
         ),
         out_shape=[
-            jax.ShapeDtypeStruct(routes.shape, jnp.int32),
+            jax.ShapeDtypeStruct(by_choice.shape, jnp.int32),
             jax.ShapeDtypeStruct((slot_total, cols_part), BF),
         ],
         compiler_params=pltpu.CompilerParams(vmem_limit_bytes=12 * 1024 * 1024),
-    )(me.reshape(1), routes, token_rows)
+    )(me.reshape(1), by_choice, token_rows)
     outgoing, conv_input, in_gate = lax.optimization_barrier((outgoing, conv_input, in_gate))
     arrived = lax.all_to_all(
         outgoing.reshape(depth, 2, capacity, cols_part), "z", 0, 0, tiled=True
@@ -259,7 +260,6 @@
     after = step(gated, -1, 0)
     far = step(gated, 2, 0)
     line = jnp.concatenate([gated, after, far, before], axis=0)
-    arrived, line = lax.optimization_barrier((arrived, line))
 
     def exchange(value, groups):
         return lax.all_to_all(
@@ -269,9 +269,10 @@
     rows_own = arrived[:, 0].reshape(half, cols_part)
     rows_other = lax.ppermute(arrived[:, 1].reshape(half, cols_part), "c", swap)
     rows = jnp.concatenate([rows_own, rows_other], axis=0)
-    x = lax.all_to_all(
-        jnp.broadcast_to(rows[None], (tp,) + rows.shape), "tp", 0, 0, tiled=True
-    )
+    quarter = exchange(jnp.broadcast_to(rows[None], (side,) + rows.shape), early)
+    quarter, line = lax.optimization_barrier((quarter, line))
+    x = exchange(jnp.broadcast_to(quarter[None], (side,) + quarter.shape), late)
+    x = x.reshape(tp, slot_total, cols_part)
     weights = (expert_gate[0], expert_up[0], expert_down[0])
     part = expert_part(me, x, *weights, rows_b)
     part = part.reshape(side, side, slot_total, cols_part)

time: 195 us -> 185 us (0.949)
  blocking collectives: 86.3 us -> 59.9 us
  waiting for transfers between devices: 17.7 us -> 26.2 us
  starting transfers between devices: 63 us -> 71.3 us
    all_to_all x1 -> x0, blocking collectives: 56.9 us -> none  [layer(): lax.all_to_all(jnp.broadcast_to(rows[None], (tp,) + rows.shape), 'tp', 0,...]
    all_to_all x1 -> x2, blocking collectives: 29.5 us -> 59.9 us  [exchange(): lax.all_to_all(value, ('c', 'tp'), 0, 0, axis_index_groups=groups, tiled=...]
    all_to_all x1, waiting for transfers between devices: 0.01 us -> 8.12 us  [layer(): lax.all_to_all(outgoing.reshape(depth, 2, capacity, cols_part), 'z', 0, 0...]
    ppermute x1, starting transfers between devices: 2.51 us -> 8.12 us  [layer(): rows_other = lax.ppermute(arrived[:, 1].reshape(half, cols_part), 'c', swap)]
    all_to_all x1, starting transfers between devices: 9.78 us -> 5.01 us  [layer(): returned = lax.all_to_all(back, 'z', 0, 0, tiled=True)]
    all_to_all x1 -> x2, starting transfers between devices: 3.65 us -> 7.83 us  [exchange(): lax.all_to_all(value, ('c', 'tp'), 0, 0, axis_index_groups=groups, tiled=...]
    ppermute x1, starting transfers between devices: 5.66 us -> 7.67 us  [layer(): back_other = lax.ppermute(expert_rows[half:], 'c', swap)]
  transfers between devices with their start and end apart: 13 -> 14, of which waited for: 7 -> 9; matrix products, arithmetic and copies ran while one was open for 3% -> 3% of each run, Pallas kernels for 2% -> 2%
where the time goes in v3:
time: 185 us; the launch traced here: 182 us
  starting transfers between devices  71.3 us (39%)
  blocking collectives  59.9 us (32%)
  waiting for transfers between devices  26.2 us (14%)
  Pallas kernels  15 us (8%)
  local copies, waits for them, and re-layouts  6.54 us (4%)
  other arithmetic  2.48 us (1%)
    all_to_all x2, blocking collectives, exchange(): lax.all_to_all(value, ('c', 'tp'), 0, 0, axis_index_groups=groups, tiled=...  59.9 us
    ppermute x7, starting transfers between devices, step(): return lax.ppermute(value, ('c', 'tp'), pairs)  22.5 us
    all_to_all x1, starting transfers between devices, layer(): lax.all_to_all(outgoing.reshape(depth, 2, capacity, cols_part), 'z', 0, 0...  15.7 us
    ppermute x7, waiting for transfers between devices, step(): return lax.ppermute(value, ('c', 'tp'), pairs)  13 us
    ppermute x1, starting transfers between devices, layer(): rows_other = lax.ppermute(arrived[:, 1].reshape(half, cols_part), 'c', swap)  8.12 us
    all_to_all x1, waiting for transfers between devices, layer(): lax.all_to_all(outgoing.reshape(depth, 2, capacity, cols_part), 'z', 0, 0...  8.12 us
    all_to_all x2, starting transfers between devices, exchange(): lax.all_to_all(value, ('c', 'tp'), 0, 0, axis_index_groups=groups, tiled=...  7.83 us
    ppermute x1, starting transfers between devices, layer(): back_other = lax.ppermute(expert_rows[half:], 'c', swap)  7.67 us
  transfers between devices with their start and end apart: 14, of which 9 were waited for; matrix products, arithmetic and copies ran while one was open for 3% of the time, Pallas kernels for 2%

profile of v3, /device:TPU:1, one launch (start us, length us, event | category | flops | bytes accessed | tf_op | source)
XLA Modules:
  0.0 182.3 jit_solution(1589801192280926191)
XLA Ops:
  3.4 15.7 %all-to-all-start = ((bf16[16,2,32,128]{3,2,1,0:T(8,128)(2,1)}), bf16[16,2,32,128]{3,2,1,0:T(8,128)(2,1)S(1)}, u32[]{:S(2)}, u32[]{:S(2)}) async-start(bf16[16,2,32,128]{3,2,1,0:T(8,128)(2,1)} %bitcast.2), calls=%async_computation | async-start | bytes 524288 | tf_op jit(solution)/shard_map/all_to_all | solution.py:220
  20.3 4.4 %collective-permute-start.1 = (bf16[64,2]{1,0:T(8,128)(2,1)S(1)}, bf16[64,2]{1,0:T(8,128)(2,1)S(1)}, u32[]{:S(2)}, u32[]{:S(2)}) collective-permute-start(bf16[64,2]{1,0:T(8,128)(2,1)S(1)} %slice.54), channel_id=1, source_target_pairs={{0,16},{16,32},{32,48},{48,64},{64,80},{80,96},{96,112},{112,128},... | collective-permute-start | bytes 776 | tf_op jit(solution)/shard_map/ppermute | solution.py:230
  24.8 8.1 %all-to-all-done = bf16[16,2,32,128]{3,2,1,0:T(8,128)(2,1)S(1)} async-done(((bf16[16,2,32,128]{3,2,1,0:T(8,128)(2,1)}), bf16[16,2,32,128]{3,2,1,0:T(8,128)(2,1)S(1)}, u32[]{:S(2)}, u32[]{:S(2)}) %all-to-all-start) | async-done | bytes 262176 | tf_op jit(solution)/shard_map/all_to_all | solution.py:220
  32.9 8.1 %collective-permute-start = (bf16[512,128]{1,0:T(8,128)(2,1)S(1)}, bf16[512,128]{1,0:T(8,128)(2,1)S(1)}, u32[]{:S(2)}, u32[]{:S(2)}) collective-permute-start(bf16[512,128]{1,0:T(8,128)(2,1)S(1)} %bitcast.42), channel_id=1, source_target_pairs={{0,16},{16,0},{1,17},{17,1},{2,18},{18,2},{3,19},{19,3},{4,20},{20... | collective-permute-start | bytes 393224 | tf_op jit(solution)/shard_map/ppermute | solution.py:270
  43.2 4.2 %all-to-all-start.1 = ((bf16[4,1024,128]{2,1,0:T(8,128)(2,1)}), bf16[4,1024,128]{2,1,0:T(8,128)(2,1)S(1)}, u32[]{:S(2)}, u32[]{:S(2)}) async-start(bf16[4,1024,128]{2,1,0:T(8,128)(2,1)} %broadcast_in_dim.4), calls=%async_computation.1 | async-start | bytes 2097152 | tf_op jit(solution)/shard_map/all_to_all | solution.py:265
  47.7 4.6 %collective-permute-start.2 = (bf16[2,32,2048]{2,1,0:T(8,128)(2,1)S(1)}, bf16[2,32,2048]{2,1,0:T(8,128)(2,1)S(1)}, u32[]{:S(2)}, u32[]{:S(2)}) collective-permute-start(bf16[2,32,2048]{2,1,0:T(8,128)(2,1)S(1)} %bitcast.36), channel_id=1, source_target_pairs={{0,3},{1,0},{2,1},{3,2},{4,7},{5,4},{6,5},{7,6},{8,11},{9,8},{10,9... | collective-permute-start | bytes 786440 | tf_op jit(solution)/shard_map/ppermute | solution.py:256
  52.3 2.5 %collective-permute-start.3 = (bf16[2,32,2048]{2,1,0:T(8,128)(2,1)S(1)}, bf16[2,32,2048]{2,1,0:T(8,128)(2,1)S(1)}, u32[]{:S(2)}, u32[]{:S(2)}) collective-permute-start(bf16[2,32,2048]{2,1,0:T(8,128)(2,1)S(1)} %bitcast.37), channel_id=1, source_target_pairs={{0,2},{1,3},{2,0},{3,1},{4,6},{5,7},{6,4},{7,5},{8,10},{9,11},{10,... | collective-permute-start | bytes 786440 | tf_op jit(solution)/shard_map/ppermute | solution.py:256
  54.8 2.5 %collective-permute-start.4 = (bf16[2,32,2048]{2,1,0:T(8,128)(2,1)S(1)}, bf16[2,32,2048]{2,1,0:T(8,128)(2,1)S(1)}, u32[]{:S(2)}, u32[]{:S(2)}) collective-permute-start(bf16[2,32,2048]{2,1,0:T(8,128)(2,1)S(1)} %bitcast.38), channel_id=1, source_target_pairs={{0,1},{1,2},{2,3},{3,0},{4,5},{5,6},{6,7},{7,4},{8,9},{9,10},{10,1... | collective-permute-start | bytes 786440 | tf_op jit(solution)/shard_map/ppermute | solution.py:256
  58.7 2.5 %collective-permute-done.3 = bf16[2,32,2048]{2,1,0:T(8,128)(2,1)S(1)} collective-permute-done((bf16[2,32,2048]{2,1,0:T(8,128)(2,1)S(1)}, bf16[2,32,2048]{2,1,0:T(8,128)(2,1)S(1)}, u32[]{:S(2)}, u32[]{:S(2)}) %collective-permute-start.3) | collective-permute-done | bytes 262176 | tf_op jit(solution)/shard_map/ppermute | solution.py:256
  61.2 2.8 %collective-permute-done.4 = bf16[2,32,2048]{2,1,0:T(8,128)(2,1)S(1)} collective-permute-done((bf16[2,32,2048]{2,1,0:T(8,128)(2,1)S(1)}, bf16[2,32,2048]{2,1,0:T(8,128)(2,1)S(1)}, u32[]{:S(2)}, u32[]{:S(2)}) %collective-permute-start.4) | collective-permute-done | bytes 262176 | tf_op jit(solution)/shard_map/ppermute | solution.py:256
  65.0 30.7 %all_to_all.30 = bf16[4,4,1024,128]{3,2,1,0:T(8,128)(2,1)S(1)} all-to-all(bf16[4,4,1024,128]{3,2,1,0:T(8,128)(2,1)S(1)} %broadcast_in_dim.5), channel_id=1, replica_groups={{0,4,8,12},{1,5,9,13},{2,6,10,14},{3,7,11,15},{16,17,18,19},{20,21,22,2..., dimensions={0} | all-to-all | bytes 8388608 | tf_op jit(solution)/shard_map/all_to_all | solution.py:265
  95.7 5.0 %shard_map.123 = bf16[16,1024,128]{2,1,0:T(8,128)(2,1)S(1)} custom-call(s32[1]{0:T(128)} %bitcast.me_ref, bf16[16,1024,128]{2,1,0:T(8,128)(2,1)S(1)} %bitcast.28, bf16[2048,256]{1,0:T(8,128)(2,1)S(1)} %bitcast.33, bf16[2048,256]{1,0:T(8,128)(2,1)S(1)} %bitcast.34, bf16[256,2048]{1,0:T(8,128)(2,1)S(1)} %bitcast.35), custom_call_target="tpu_custom_call" | custom-call | flops 3221225472 | bytes 11534336 | tf_op jit(solution)/shard_map/pallas_call | solution.py:91
  100.7 29.2 %all_to_all.31 = bf16[4,4,1024,128]{3,2,1,0:T(8,128)(2,1)S(1)} all-to-all(bf16[4,4,1024,128]{3,2,1,0:T(8,128)(2,1)S(1)} %bitcast.29), channel_id=1, replica_groups={{0,1,2,3},{4,5,6,7},{8,9,10,11},{12,13,14,15},{16,20,24,28},{17,21,25,2..., dimensions={0} | all-to-all | bytes 8388608 | tf_op jit(solution)/shard_map/all_to_all | solution.py:265
  129.9 3.2 %shard_map.124 = bf16[4096,128]{1,0:T(8,128)(2,1)} custom-call(bf16[4,4096,128]{2,1,0:T(8,128)(2,1)S(1)} %bitcast.27), custom_call_target="tpu_custom_call" | custom-call | tf_op jit(solution)/shard_map/pallas_call | solution.py:166
  133.1 3.6 %all-to-all-start.4 = ((bf16[4,1024,128]{2,1,0:T(8,128)(2,1)}), bf16[4,1024,128]{2,1,0:T(8,128)(2,1)S(1)}, u32[]{:S(2)}, u32[]{:S(2)}) async-start(bf16[4,1024,128]{2,1,0:T(8,128)(2,1)} %bitcast.15), calls=%async_computation.4 | async-start | bytes 2097152 | tf_op jit(solution)/shard_map/all_to_all | solution.py:265
  136.8 3.3 %collective-permute-start.7 = (bf16[8,32,2048]{2,1,0:T(8,128)(2,1)S(1)}, bf16[8,32,2048]{2,1,0:T(8,128)(2,1)S(1)}, u32[]{:S(2)}, u32[]{:S(2)}) collective-permute-start(bf16[8,32,2048]{2,1,0:T(8,128)(2,1)S(1)} %pad_maximum_fusion.y0_ref), channel_id=1, source_target_pairs={{0,4},{1,5},{2,6},{3,7},{4,8},{5,9},{6,10},{7,11},{8,12},{9,13},{1... | collective-permute-start | bytes 3145736 | tf_op jit(solution)/shard_map/ppermute | solution.py:256
  140.1 3.2 %collective-permute-start.6 = (bf16[8,32,2048]{2,1,0:T(8,128)(2,1)S(1)}, bf16[8,32,2048]{2,1,0:T(8,128)(2,1)}, u32[]{:S(2)}, u32[]{:S(2)}) collective-permute-start(bf16[8,32,2048]{2,1,0:T(8,128)(2,1)S(1)} %pad_maximum_fusion.y0_ref), channel_id=1, source_target_pairs={{0,12},{1,13},{2,14},{3,15},{4,0},{5,1},{6,2},{7,3},{8,4},{9,5},{1... | collective-permute-start | bytes 3145736 | tf_op jit(solution)/shard_map/ppermute | solution.py:256
  143.3 3.3 %all-to-all-done.4.in_ref = bf16[4,1024,128]{2,1,0:T(8,128)(2,1)S(1)} async-done(((bf16[4,1024,128]{2,1,0:T(8,128)(2,1)}), bf16[4,1024,128]{2,1,0:T(8,128)(2,1)S(1)}, u32[]{:S(2)}, u32[]{:S(2)}) %all-to-all-start.4) | async-done | bytes 1048608 | tf_op jit(solution)/shard_map/all_to_all | solution.py:265
  146.9 7.7 %collective-permute-start.5 = (bf16[512,128]{1,0:T(8,128)(2,1)S(1)}, bf16[512,128]{1,0:T(8,128)(2,1)S(1)}, u32[]{:S(2)}, u32[]{:S(2)}) collective-permute-start(bf16[512,128]{1,0:T(8,128)(2,1)S(1)} %get-tuple-element.25), channel_id=1, source_target_pairs={{0,16},{16,0},{1,17},{17,1},{2,18},{18,2},{3,19},{19,3},{4,20},{20... | collective-permute-start | bytes 393224 | tf_op jit(solution)/shard_map/ppermute | solution.py:287
  156.2 5.0 %all-to-all-start.5 = ((bf16[16,2,32,128]{3,2,1,0:T(8,128)(2,1)}), bf16[16,2,32,128]{3,2,1,0:T(8,128)(2,1)S(1)}, u32[]{:S(2)}, u32[]{:S(2)}) async-start(bf16[16,2,32,128]{3,2,1,0:T(8,128)(2,1)} %pad_maximum_fusion.2), calls=%async_computation.5 | async-start | bytes 524288 | tf_op jit(solution)/shard_map/all_to_all | solution.py:297
  166.2 4.3 %collective-permute-start.9 = (bf16[4,32,2048]{2,1,0:T(8,128)(2,1)}, bf16[4,32,2048]{2,1,0:T(8,128)(2,1)}, u32[]{:S(2)}, u32[]{:S(2)}) collective-permute-start(bf16[4,32,2048]{2,1,0:T(8,128)(2,1)} %slice.61), channel_id=1, source_target_pairs={{0,12},{1,13},{2,14},{3,15},{4,0},{5,1},{6,2},{7,3},{8,4},{9,5},{1... | collective-permute-start | bytes 1572872 | tf_op jit(solution)/shard_map/ppermute | solution.py:256
  170.6 3.1 %collective-permute-done.8.y2a_ref = bf16[4,32,2048]{2,1,0:T(8,128)(2,1)S(1)} collective-permute-done((bf16[4,32,2048]{2,1,0:T(8,128)(2,1)}, bf16[4,32,2048]{2,1,0:T(8,128)(2,1)S(1)}, u32[]{:S(2)}, u32[]{:S(2)}) %collective-permute-start.8) | collective-permute-done | bytes 524320 | tf_op jit(solution)/shard_map/ppermute | solution.py:256
  173.7 3.2 %collective-permute-done.9.y2b_ref = bf16[4,32,2048]{2,1,0:T(8,128)(2,1)} collective-permute-done((bf16[4,32,2048]{2,1,0:T(8,128)(2,1)}, bf16[4,32,2048]{2,1,0:T(8,128)(2,1)}, u32[]{:S(2)}, u32[]{:S(2)}) %collective-permute-start.9) | collective-permute-done | bytes 524320 | tf_op jit(solution)/shard_map/ppermute | solution.py:256
  176.9 4.2 %shard_map.126 = bf16[2048,128]{1,0:T(8,128)(2,1)} custom-call(s32[1]{0:T(128)} %bitcast.me_ref, bf16[8,32,2048]{2,1,0:T(8,128)(2,1)S(1)} %pad_maximum_fusion.y0_ref, bf16[8,32,2048]{2,1,0:T(8,128)(2,1)} %collective-permute-done.6.y1_ref, bf16[4,32,2048]{2,1,0:T(8,128)(2,1)S(1)} %collective-permute-done.8.y2a_ref, ...), custom_call_target="tpu_custom_call" | custom-call | flops 536870912 | bytes 4980736 | tf_op jit(solution)/shard_map/pallas_call | solution.py:143
  (46 shorter events, 17.0 us)
Async XLA Ops:
  0.6 24.1 %copy-start = (f32[3,1024]{1,0:T(4,128)S(1)}, f32[3,1024]{1,0:T(4,128)}, u32[]{:S(2)}) copy-start(f32[3,1024]{1,0:T(4,128)} %param.14) | copy-start | bytes 36868
  0.7 0.8 copy-start.2
  1.5 0.7 copy-start.3
  2.2 45.2 %copy-start.7 = (bf16[64,2048]{1,0:T(8,128)(2,1)S(1)}, bf16[64,2048]{1,0:T(8,128)(2,1)}, u32[]{:S(2)}) copy-start(bf16[64,2048]{1,0:T(8,128)(2,1)} %param.12) | copy-start | bytes 786436
  3.4 29.5 %all-to-all-start = ((bf16[16,2,32,128]{3,2,1,0:T(8,128)(2,1)}), bf16[16,2,32,128]{3,2,1,0:T(8,128)(2,1)S(1)}, u32[]{:S(2)}, u32[]{:S(2)}) async-start(bf16[16,2,32,128]{3,2,1,0:T(8,128)(2,1)} %bitcast.2), calls=%async_computation | async-start | bytes 524288 | tf_op jit(solution)/shard_map/all_to_all | solution.py:220
  20.3 20.8 %collective-permute-start.1 = (bf16[64,2]{1,0:T(8,128)(2,1)S(1)}, bf16[64,2]{1,0:T(8,128)(2,1)S(1)}, u32[]{:S(2)}, u32[]{:S(2)}) collective-permute-start(bf16[64,2]{1,0:T(8,128)(2,1)S(1)} %slice.54), channel_id=1, source_target_pairs={{0,16},{16,32},{32,48},{48,64},{64,80},{80,96},{96,112},{112,128},... | collective-permute-start | bytes 776 | tf_op jit(solution)/shard_map/ppermute | solution.py:230
  32.9 9.1 %collective-permute-start = (bf16[512,128]{1,0:T(8,128)(2,1)S(1)}, bf16[512,128]{1,0:T(8,128)(2,1)S(1)}, u32[]{:S(2)}, u32[]{:S(2)}) collective-permute-start(bf16[512,128]{1,0:T(8,128)(2,1)S(1)} %bitcast.42), channel_id=1, source_target_pairs={{0,16},{16,0},{1,17},{17,1},{2,18},{18,2},{3,19},{19,3},{4,20},{20... | collective-permute-start | bytes 393224 | tf_op jit(solution)/shard_map/ppermute | solution.py:270
  43.2 21.0 %all-to-all-start.1 = ((bf16[4,1024,128]{2,1,0:T(8,128)(2,1)}), bf16[4,1024,128]{2,1,0:T(8,128)(2,1)S(1)}, u32[]{:S(2)}, u32[]{:S(2)}) async-start(bf16[4,1024,128]{2,1,0:T(8,128)(2,1)} %broadcast_in_dim.4), calls=%async_computation.1 | async-start | bytes 2097152 | tf_op jit(solution)/shard_map/all_to_all | solution.py:265
  47.7 11.0 %collective-permute-start.2 = (bf16[2,32,2048]{2,1,0:T(8,128)(2,1)S(1)}, bf16[2,32,2048]{2,1,0:T(8,128)(2,1)S(1)}, u32[]{:S(2)}, u32[]{:S(2)}) collective-permute-start(bf16[2,32,2048]{2,1,0:T(8,128)(2,1)S(1)} %bitcast.36), channel_id=1, source_target_pairs={{0,3},{1,0},{2,1},{3,2},{4,7},{5,4},{6,5},{7,6},{8,11},{9,8},{10,9... | collective-permute-start | bytes 786440 | tf_op jit(solution)/shard_map/ppermute | solution.py:256
  52.3 8.9 %collective-permute-start.3 = (bf16[2,32,2048]{2,1,0:T(8,128)(2,1)S(1)}, bf16[2,32,2048]{2,1,0:T(8,128)(2,1)S(1)}, u32[]{:S(2)}, u32[]{:S(2)}) collective-permute-start(bf16[2,32,2048]{2,1,0:T(8,128)(2,1)S(1)} %bitcast.37), channel_id=1, source_target_pairs={{0,2},{1,3},{2,0},{3,1},{4,6},{5,7},{6,4},{7,5},{8,10},{9,11},{10,... | collective-permute-start | bytes 786440 | tf_op jit(solution)/shard_map/ppermute | solution.py:256
  54.8 9.2 %collective-permute-start.4 = (bf16[2,32,2048]{2,1,0:T(8,128)(2,1)S(1)}, bf16[2,32,2048]{2,1,0:T(8,128)(2,1)S(1)}, u32[]{:S(2)}, u32[]{:S(2)}) collective-permute-start(bf16[2,32,2048]{2,1,0:T(8,128)(2,1)S(1)} %bitcast.38), channel_id=1, source_target_pairs={{0,1},{1,2},{2,3},{3,0},{4,5},{5,6},{6,7},{7,4},{8,9},{9,10},{10,1... | collective-permute-start | bytes 786440 | tf_op jit(solution)/shard_map/ppermute | solution.py:256
  65.0 30.7 %copy-start.4 = (bf16[1,2048,256]{2,1,0:T(8,128)(2,1)S(1)}, bf16[1,2048,256]{2,1,0:T(8,128)(2,1)}, u32[]{:S(2)}) copy-start(bf16[1,2048,256]{2,1,0:T(8,128)(2,1)} %param.19) | copy-start | bytes 3145732
  65.0 30.7 %copy-start.5 = (bf16[1,2048,256]{2,1,0:T(8,128)(2,1)S(1)}, bf16[1,2048,256]{2,1,0:T(8,128)(2,1)}, u32[]{:S(2)}) copy-start(bf16[1,2048,256]{2,1,0:T(8,128)(2,1)} %param.20) | copy-start | bytes 3145732
  65.0 30.7 %copy-start.6 = (bf16[1,256,2048]{2,1,0:T(8,128)(2,1)S(1)}, bf16[1,256,2048]{2,1,0:T(8,128)(2,1)}, u32[]{:S(2)}) copy-start(bf16[1,256,2048]{2,1,0:T(8,128)(2,1)} %param.21) | copy-start | bytes 3145732
  133.1 37.4 %copy-start.8 = (f32[256,2]{0,1:T(2,128)S(1)}, f32[256,2]{0,1:T(2,128)}, u32[]{:S(2)}) copy-start(f32[256,2]{0,1:T(2,128)} %param.18) | copy-start | bytes 6148
  133.1 43.8 %copy-start.1 = (bf16[1024,128]{1,0:T(8,128)(2,1)S(1)}, bf16[1024,128]{1,0:T(8,128)(2,1)}, u32[]{:S(2)}) copy-start(bf16[1024,128]{1,0:T(8,128)(2,1)} %param.15) | copy-start | bytes 786436
  133.1 13.5 %all-to-all-start.4 = ((bf16[4,1024,128]{2,1,0:T(8,128)(2,1)}), bf16[4,1024,128]{2,1,0:T(8,128)(2,1)S(1)}, u32[]{:S(2)}, u32[]{:S(2)}) async-start(bf16[4,1024,128]{2,1,0:T(8,128)(2,1)} %bitcast.15), calls=%async_computation.4 | async-start | bytes 2097152 | tf_op jit(solution)/shard_map/all_to_all | solution.py:265
  136.8 24.5 %collective-permute-start.7 = (bf16[8,32,2048]{2,1,0:T(8,128)(2,1)S(1)}, bf16[8,32,2048]{2,1,0:T(8,128)(2,1)S(1)}, u32[]{:S(2)}, u32[]{:S(2)}) collective-permute-start(bf16[8,32,2048]{2,1,0:T(8,128)(2,1)S(1)} %pad_maximum_fusion.y0_ref), channel_id=1, source_target_pairs={{0,4},{1,5},{2,6},{3,7},{4,8},{5,9},{6,10},{7,11},{8,12},{9,13},{1... | collective-permute-start | bytes 3145736 | tf_op jit(solution)/shard_map/ppermute | solution.py:256
  140.1 24.2 %collective-permute-start.6 = (bf16[8,32,2048]{2,1,0:T(8,128)(2,1)S(1)}, bf16[8,32,2048]{2,1,0:T(8,128)(2,1)}, u32[]{:S(2)}, u32[]{:S(2)}) collective-permute-start(bf16[8,32,2048]{2,1,0:T(8,128)(2,1)S(1)} %pad_maximum_fusion.y0_ref), channel_id=1, source_target_pairs={{0,12},{1,13},{2,14},{3,15},{4,0},{5,1},{6,2},{7,3},{8,4},{9,5},{1... | collective-permute-start | bytes 3145736 | tf_op jit(solution)/shard_map/ppermute | solution.py:256
  146.9 8.6 %collective-permute-start.5 = (bf16[512,128]{1,0:T(8,128)(2,1)S(1)}, bf16[512,128]{1,0:T(8,128)(2,1)S(1)}, u32[]{:S(2)}, u32[]{:S(2)}) collective-permute-start(bf16[512,128]{1,0:T(8,128)(2,1)S(1)} %get-tuple-element.25), channel_id=1, source_target_pairs={{0,16},{16,0},{1,17},{17,1},{2,18},{18,2},{3,19},{19,3},{4,20},{20... | collective-permute-start | bytes 393224 | tf_op jit(solution)/shard_map/ppermute | solution.py:287
  156.2 24.9 %all-to-all-start.5 = ((bf16[16,2,32,128]{3,2,1,0:T(8,128)(2,1)}), bf16[16,2,32,128]{3,2,1,0:T(8,128)(2,1)S(1)}, u32[]{:S(2)}, u32[]{:S(2)}) async-start(bf16[16,2,32,128]{3,2,1,0:T(8,128)(2,1)} %pad_maximum_fusion.2), calls=%async_computation.5 | async-start | bytes 524288 | tf_op jit(solution)/shard_map/all_to_all | solution.py:297
  162.1 11.6 %collective-permute-start.8 = (bf16[4,32,2048]{2,1,0:T(8,128)(2,1)}, bf16[4,32,2048]{2,1,0:T(8,128)(2,1)S(1)}, u32[]{:S(2)}, u32[]{:S(2)}) collective-permute-start(bf16[4,32,2048]{2,1,0:T(8,128)(2,1)} %slice.60), channel_id=1, source_target_pairs={{0,4},{1,5},{2,6},{3,7},{4,8},{5,9},{6,10},{7,11},{8,12},{9,13},{1... | collective-permute-start | bytes 1572872 | tf_op jit(solution)/shard_map/ppermute | solution.py:256
  166.2 10.7 %collective-permute-start.9 = (bf16[4,32,2048]{2,1,0:T(8,128)(2,1)}, bf16[4,32,2048]{2,1,0:T(8,128)(2,1)}, u32[]{:S(2)}, u32[]{:S(2)}) collective-permute-start(bf16[4,32,2048]{2,1,0:T(8,128)(2,1)} %slice.61), channel_id=1, source_target_pairs={{0,12},{1,13},{2,14},{3,15},{4,0},{5,1},{6,2},{7,3},{8,4},{9,5},{1... | collective-permute-start | bytes 1572872 | tf_op jit(solution)/shard_map/ppermute | solution.py:256

commit v4 on v3

--- a/solution.py
+++ b/solution.py
@@ -111,54 +111,60 @@
     )(me.reshape(1), x, gate_weight, up_weight, down_weight)
 
 
-def mixer_kernel(me_ref, y0_ref, y1_ref, y2a_ref, y2b_ref, y3_ref, proj_ref, out_ref):
+def mixer_kernel(me_ref, *refs, fars, last):
+    refs, out_ref = refs[:-1], refs[-1]
+    proj_ref, refs = refs[0], refs[1:]
     blocks = proj_ref.shape[0]
     side = 4
     core = me_ref[0] // blocks
     row = (me_ref[0] % blocks) // side
     col = me_ref[0] % side
     weights = []
-    for far in range(side):
+    for far in fars:
         for near in range(side):
             down = jnp.where(core == 0, far, near)
             right = jnp.where(core == 0, near, far)
             at = ((row + down) % side) * side + (col + right) % side
             weights.append(proj_ref[at])
     proj = jnp.concatenate(weights, axis=0)
-    pieces = [
-        ref[i]
-        for ref in (y0_ref, y1_ref, y2a_ref, y2b_ref, y3_ref)
-        for i in range(ref.shape[0])
-    ]
-    y = jnp.concatenate(pieces, axis=0)
+    pieces = refs[:-1] if last else refs
+    y = jnp.concatenate([ref[i] for ref in pieces for i in range(ref.shape[0])], axis=0)
     flat = lax.dot_general(
         proj, y, (((0,), (0,)), ((), ())), preferred_element_type=F32
     )
-    out_ref[...] = jnp.transpose(flat).astype(BF)
-
-
-def mixer_product(me, pieces, proj, tile):
+    if last:
+        out_ref[...] = jnp.transpose(flat + refs[-1][...]).astype(BF)
+    else:
+        out_ref[...] = flat
+
+
+def mixer_product(me, proj, pieces, fars, base, tile):
     length = pieces[0].shape[2]
-    blocks, width, cols = proj.shape
+    _, width, cols = proj.shape
+    last = base is not None
+    flat_spec = pl.BlockSpec((cols, tile), lambda i, c: (0, i))
     return pl.pallas_call(
-        mixer_kernel,
+        functools.partial(mixer_kernel, fars=fars, last=last),
         grid_spec=pltpu.PrefetchScalarGridSpec(
             num_scalar_prefetch=1,
             grid=(length // tile,),
-            in_specs=[
+            in_specs=[pl.BlockSpec(proj.shape, lambda i, c: (0, 0, 0))]
+            + [
                 pl.BlockSpec(p.shape[:2] + (tile,), lambda i, c: (0, 0, i)) for p in pieces
             ]
-            + [pl.BlockSpec(proj.shape, lambda i, c: (0, 0, 0))],
-            out_specs=pl.BlockSpec((tile, cols), lambda i, c: (i, 0)),
-        ),
-        out_shape=jax.ShapeDtypeStruct((length, cols), BF),
-        compiler_params=pltpu.CompilerParams(vmem_limit_bytes=20 * 1024 * 1024),
+            + ([flat_spec] if last else []),
+            out_specs=pl.BlockSpec((tile, cols), lambda i, c: (i, 0)) if last else flat_spec,
+        ),
+        out_shape=jax.ShapeDtypeStruct((length, cols), BF)
+        if last
+        else jax.ShapeDtypeStruct((cols, length), F32),
+        compiler_params=pltpu.CompilerParams(vmem_limit_bytes=16 * 1024 * 1024),
         cost_estimate=pl.CostEstimate(
-            flops=2 * length * blocks * width * cols,
-            bytes_accessed=2 * length * (blocks * width + cols) + 2 * proj.size,
+            flops=2 * length * len(fars) * 4 * width * cols,
+            bytes_accessed=2 * length * (len(fars) * 4 * width + 2 * cols) + 2 * proj.size,
             transcendentals=0,
         ),
-    )(me.reshape(1), *pieces, proj)
+    )(me.reshape(1), proj, *pieces, *([base] if last else []))
 
 
 def sum_parts(arrived, steps):
@@ -217,9 +223,7 @@
         compiler_params=pltpu.CompilerParams(vmem_limit_bytes=12 * 1024 * 1024),
     )(me.reshape(1), by_choice, token_rows)
     outgoing, conv_input, in_gate = lax.optimization_barrier((outgoing, conv_input, in_gate))
-    arrived = lax.all_to_all(
-        outgoing.reshape(depth, 2, capacity, cols_part), "z", 0, 0, tiled=True
-    )
+    arrived = lax.all_to_all(outgoing.reshape(depth, 2, capacity, cols_part), "z", 0, 0, tiled=True)
 
     length = conv_input.shape[1]
     width_part = conv_input.shape[0]
@@ -295,11 +299,12 @@
     line_far_a = step(line_before[:4], 1, 1)
     line_far_b = step(line_after[4:], -1, 1)
     returned = lax.all_to_all(back, "z", 0, 0, tiled=True)
+    blocks = mixer_proj.reshape(tp, width_part, cols_part)
+    most = mixer_product(
+        me, blocks, (line, line_after, line_before), (0, 1, 3), None, length // 4
+    )
     mixed_out = mixer_product(
-        me,
-        (line, line_after, line_far_a, line_far_b, line_before),
-        mixer_proj.reshape(tp, width_part, cols_part),
-        length // 4,
+        me, blocks, (line_far_a, line_far_b), (2,), most, length // 4
     )
     returned, mixed_out = lax.optimization_barrier((returned, mixed_out))
     returned = returned.reshape(slot_total, cols_part)

time: 185 us -> 185 us (level)
  waiting for transfers between devices: 26.2 us -> 23.1 us
  Pallas kernels: 15 us -> 17.7 us
    ppermute x7, waiting for transfers between devices: 13 us -> 9.87 us  [step(): return lax.ppermute(value, ('c', 'tp'), pairs)]
    pallas_call x1 -> x2, Pallas kernels: 4.23 us -> 6.91 us  [mixer_product(): pl.pallas_call(functools.partial(mixer_kernel, fars=fars, last=last), gri...]
  transfers between devices with their start and end apart: 14 -> 14, of which waited for: 9 -> 8; matrix products, arithmetic and copies ran while one was open for 3% -> 3% of each run, Pallas kernels for 2% -> 4%
where the time goes in v4:
time: 185 us; the launch traced here: 182 us
  starting transfers between devices  71.3 us (39%)
  blocking collectives  59.9 us (32%)
  waiting for transfers between devices  23.1 us (12%)
  Pallas kernels  17.7 us (10%)
  local copies, waits for them, and re-layouts  6.56 us (4%)
  other arithmetic  2.48 us (1%)
    all_to_all x2, blocking collectives, exchange(): lax.all_to_all(value, ('c', 'tp'), 0, 0, axis_index_groups=groups, tiled=...  59.9 us
    ppermute x7, starting transfers between devices, step(): return lax.ppermute(value, ('c', 'tp'), pairs)  22.5 us
    all_to_all x1, starting transfers between devices, layer(): lax.all_to_all(outgoing.reshape(depth, 2, capacity, cols_part), 'z', 0, 0...  15.7 us
    ppermute x7, waiting for transfers between devices, step(): return lax.ppermute(value, ('c', 'tp'), pairs)  9.87 us
    ppermute x1, starting transfers between devices, layer(): rows_other = lax.ppermute(arrived[:, 1].reshape(half, cols_part), 'c', swap)  8.12 us
    all_to_all x1, waiting for transfers between devices, layer(): lax.all_to_all(outgoing.reshape(depth, 2, capacity, cols_part), 'z', 0, 0...  8.12 us
    all_to_all x2, starting transfers between devices, exchange(): lax.all_to_all(value, ('c', 'tp'), 0, 0, axis_index_groups=groups, tiled=...  7.83 us
    ppermute x1, starting transfers between devices, layer(): back_other = lax.ppermute(expert_rows[half:], 'c', swap)  7.67 us
  transfers between devices with their start and end apart: 14, of which 8 were waited for; matrix products, arithmetic and copies ran while one was open for 3% of the time, Pallas kernels for 4%

profile of v4, /device:TPU:1, one launch (start us, length us, event | category | flops | bytes accessed | tf_op | source)
XLA Modules:
  0.0 181.8 jit_solution(44994628829740896)
XLA Ops:
  3.4 15.7 %all-to-all-start = ((bf16[16,2,32,128]{3,2,1,0:T(8,128)(2,1)}), bf16[16,2,32,128]{3,2,1,0:T(8,128)(2,1)S(1)}, u32[]{:S(2)}, u32[]{:S(2)}) async-start(bf16[16,2,32,128]{3,2,1,0:T(8,128)(2,1)} %bitcast.2), calls=%async_computation | async-start | bytes 524288 | tf_op jit(solution)/shard_map/all_to_all | solution.py:226
  20.3 4.4 %collective-permute-start.1 = (bf16[64,2]{1,0:T(8,128)(2,1)S(1)}, bf16[64,2]{1,0:T(8,128)(2,1)S(1)}, u32[]{:S(2)}, u32[]{:S(2)}) collective-permute-start(bf16[64,2]{1,0:T(8,128)(2,1)S(1)} %slice.54), channel_id=1, source_target_pairs={{0,16},{16,32},{32,48},{48,64},{64,80},{80,96},{96,112},{112,128},... | collective-permute-start | bytes 776 | tf_op jit(solution)/shard_map/ppermute | solution.py:234
  24.8 8.1 %all-to-all-done = bf16[16,2,32,128]{3,2,1,0:T(8,128)(2,1)S(1)} async-done(((bf16[16,2,32,128]{3,2,1,0:T(8,128)(2,1)}), bf16[16,2,32,128]{3,2,1,0:T(8,128)(2,1)S(1)}, u32[]{:S(2)}, u32[]{:S(2)}) %all-to-all-start) | async-done | bytes 262176 | tf_op jit(solution)/shard_map/all_to_all | solution.py:226
  32.9 8.1 %collective-permute-start = (bf16[512,128]{1,0:T(8,128)(2,1)S(1)}, bf16[512,128]{1,0:T(8,128)(2,1)S(1)}, u32[]{:S(2)}, u32[]{:S(2)}) collective-permute-start(bf16[512,128]{1,0:T(8,128)(2,1)S(1)} %bitcast.43), channel_id=1, source_target_pairs={{0,16},{16,0},{1,17},{17,1},{2,18},{18,2},{3,19},{19,3},{4,20},{20... | collective-permute-start | bytes 393224 | tf_op jit(solution)/shard_map/ppermute | solution.py:274
  43.2 4.2 %all-to-all-start.1 = ((bf16[4,1024,128]{2,1,0:T(8,128)(2,1)}), bf16[4,1024,128]{2,1,0:T(8,128)(2,1)S(1)}, u32[]{:S(2)}, u32[]{:S(2)}) async-start(bf16[4,1024,128]{2,1,0:T(8,128)(2,1)} %broadcast_in_dim.4), calls=%async_computation.1 | async-start | bytes 2097152 | tf_op jit(solution)/shard_map/all_to_all | solution.py:269
  47.7 4.6 %collective-permute-start.2 = (bf16[2,32,2048]{2,1,0:T(8,128)(2,1)S(1)}, bf16[2,32,2048]{2,1,0:T(8,128)(2,1)S(1)}, u32[]{:S(2)}, u32[]{:S(2)}) collective-permute-start(bf16[2,32,2048]{2,1,0:T(8,128)(2,1)S(1)} %bitcast.37), channel_id=1, source_target_pairs={{0,3},{1,0},{2,1},{3,2},{4,7},{5,4},{6,5},{7,6},{8,11},{9,8},{10,9... | collective-permute-start | bytes 786440 | tf_op jit(solution)/shard_map/ppermute | solution.py:260
  52.3 2.5 %collective-permute-start.3 = (bf16[2,32,2048]{2,1,0:T(8,128)(2,1)S(1)}, bf16[2,32,2048]{2,1,0:T(8,128)(2,1)S(1)}, u32[]{:S(2)}, u32[]{:S(2)}) collective-permute-start(bf16[2,32,2048]{2,1,0:T(8,128)(2,1)S(1)} %bitcast.38), channel_id=1, source_target_pairs={{0,2},{1,3},{2,0},{3,1},{4,6},{5,7},{6,4},{7,5},{8,10},{9,11},{10,... | collective-permute-start | bytes 786440 | tf_op jit(solution)/shard_map/ppermute | solution.py:260
  54.8 2.5 %collective-permute-start.4 = (bf16[2,32,2048]{2,1,0:T(8,128)(2,1)S(1)}, bf16[2,32,2048]{2,1,0:T(8,128)(2,1)S(1)}, u32[]{:S(2)}, u32[]{:S(2)}) collective-permute-start(bf16[2,32,2048]{2,1,0:T(8,128)(2,1)S(1)} %bitcast.39), channel_id=1, source_target_pairs={{0,1},{1,2},{2,3},{3,0},{4,5},{5,6},{6,7},{7,4},{8,9},{9,10},{10,1... | collective-permute-start | bytes 786440 | tf_op jit(solution)/shard_map/ppermute | solution.py:260
  58.7 2.5 %collective-permute-done.3 = bf16[2,32,2048]{2,1,0:T(8,128)(2,1)S(1)} collective-permute-done((bf16[2,32,2048]{2,1,0:T(8,128)(2,1)S(1)}, bf16[2,32,2048]{2,1,0:T(8,128)(2,1)S(1)}, u32[]{:S(2)}, u32[]{:S(2)}) %collective-permute-start.3) | collective-permute-done | bytes 262176 | tf_op jit(solution)/shard_map/ppermute | solution.py:260
  61.2 2.8 %collective-permute-done.4 = bf16[2,32,2048]{2,1,0:T(8,128)(2,1)S(1)} collective-permute-done((bf16[2,32,2048]{2,1,0:T(8,128)(2,1)S(1)}, bf16[2,32,2048]{2,1,0:T(8,128)(2,1)S(1)}, u32[]{:S(2)}, u32[]{:S(2)}) %collective-permute-start.4) | collective-permute-done | bytes 262176 | tf_op jit(solution)/shard_map/ppermute | solution.py:260
  65.0 30.7 %all_to_all.30 = bf16[4,4,1024,128]{3,2,1,0:T(8,128)(2,1)S(1)} all-to-all(bf16[4,4,1024,128]{3,2,1,0:T(8,128)(2,1)S(1)} %broadcast_in_dim.5), channel_id=1, replica_groups={{0,4,8,12},{1,5,9,13},{2,6,10,14},{3,7,11,15},{16,17,18,19},{20,21,22,2..., dimensions={0} | all-to-all | bytes 8388608 | tf_op jit(solution)/shard_map/all_to_all | solution.py:269
  95.7 5.0 %shard_map.123 = bf16[16,1024,128]{2,1,0:T(8,128)(2,1)S(1)} custom-call(s32[1]{0:T(128)} %bitcast.me_ref, bf16[16,1024,128]{2,1,0:T(8,128)(2,1)S(1)} %bitcast.28, bf16[2048,256]{1,0:T(8,128)(2,1)S(1)} %bitcast.34, bf16[2048,256]{1,0:T(8,128)(2,1)S(1)} %bitcast.35, bf16[256,2048]{1,0:T(8,128)(2,1)S(1)} %bitcast.36), custom_call_target="tpu_custom_call" | custom-call | flops 3221225472 | bytes 11534336 | tf_op jit(solution)/shard_map/pallas_call | solution.py:91
  100.7 29.2 %all_to_all.31 = bf16[4,4,1024,128]{3,2,1,0:T(8,128)(2,1)S(1)} all-to-all(bf16[4,4,1024,128]{3,2,1,0:T(8,128)(2,1)S(1)} %bitcast.29), channel_id=1, replica_groups={{0,1,2,3},{4,5,6,7},{8,9,10,11},{12,13,14,15},{16,20,24,28},{17,21,25,2..., dimensions={0} | all-to-all | bytes 8388608 | tf_op jit(solution)/shard_map/all_to_all | solution.py:269
  129.9 3.2 %shard_map.124 = bf16[4096,128]{1,0:T(8,128)(2,1)} custom-call(bf16[4,4096,128]{2,1,0:T(8,128)(2,1)S(1)} %bitcast.27), custom_call_target="tpu_custom_call" | custom-call | tf_op jit(solution)/shard_map/pallas_call | solution.py:172
  133.1 3.6 %all-to-all-start.4 = ((bf16[4,1024,128]{2,1,0:T(8,128)(2,1)}), bf16[4,1024,128]{2,1,0:T(8,128)(2,1)S(1)}, u32[]{:S(2)}, u32[]{:S(2)}) async-start(bf16[4,1024,128]{2,1,0:T(8,128)(2,1)} %bitcast.15), calls=%async_computation.4 | async-start | bytes 2097152 | tf_op jit(solution)/shard_map/all_to_all | solution.py:269
  136.8 3.3 %collective-permute-start.6 = (bf16[8,32,2048]{2,1,0:T(8,128)(2,1)S(1)}, bf16[8,32,2048]{2,1,0:T(8,128)(2,1)S(1)}, u32[]{:S(2)}, u32[]{:S(2)}) collective-permute-start(bf16[8,32,2048]{2,1,0:T(8,128)(2,1)S(1)} %pad_maximum_fusion.refs_1_), channel_id=1, source_target_pairs={{0,4},{1,5},{2,6},{3,7},{4,8},{5,9},{6,10},{7,11},{8,12},{9,13},{1... | collective-permute-start | bytes 3145736 | tf_op jit(solution)/shard_map/ppermute | solution.py:260
  140.1 3.2 %collective-permute-start.8 = (bf16[8,32,2048]{2,1,0:T(8,128)(2,1)S(1)}, bf16[8,32,2048]{2,1,0:T(8,128)(2,1)}, u32[]{:S(2)}, u32[]{:S(2)}) collective-permute-start(bf16[8,32,2048]{2,1,0:T(8,128)(2,1)S(1)} %pad_maximum_fusion.refs_1_), channel_id=1, source_target_pairs={{0,12},{1,13},{2,14},{3,15},{4,0},{5,1},{6,2},{7,3},{8,4},{9,5},{1... | collective-permute-start | bytes 3145736 | tf_op jit(solution)/shard_map/ppermute | solution.py:260
  143.3 3.3 %all-to-all-done.4.in_ref = bf16[4,1024,128]{2,1,0:T(8,128)(2,1)S(1)} async-done(((bf16[4,1024,128]{2,1,0:T(8,128)(2,1)}), bf16[4,1024,128]{2,1,0:T(8,128)(2,1)S(1)}, u32[]{:S(2)}, u32[]{:S(2)}) %all-to-all-start.4) | async-done | bytes 1048608 | tf_op jit(solution)/shard_map/all_to_all | solution.py:269
  146.9 7.7 %collective-permute-start.5 = (bf16[512,128]{1,0:T(8,128)(2,1)S(1)}, bf16[512,128]{1,0:T(8,128)(2,1)S(1)}, u32[]{:S(2)}, u32[]{:S(2)}) collective-permute-start(bf16[512,128]{1,0:T(8,128)(2,1)S(1)} %get-tuple-element.25), channel_id=1, source_target_pairs={{0,16},{16,0},{1,17},{17,1},{2,18},{18,2},{3,19},{19,3},{4,20},{20... | collective-permute-start | bytes 393224 | tf_op jit(solution)/shard_map/ppermute | solution.py:291
  156.2 5.0 %all-to-all-start.5 = ((bf16[16,2,32,128]{3,2,1,0:T(8,128)(2,1)}), bf16[16,2,32,128]{3,2,1,0:T(8,128)(2,1)S(1)}, u32[]{:S(2)}, u32[]{:S(2)}) async-start(bf16[16,2,32,128]{3,2,1,0:T(8,128)(2,1)} %pad_maximum_fusion.2), calls=%async_computation.5 | async-start | bytes 524288 | tf_op jit(solution)/shard_map/all_to_all | solution.py:301
  166.2 4.3 %collective-permute-start.9 = (bf16[4,32,2048]{2,1,0:T(8,128)(2,1)}, bf16[4,32,2048]{2,1,0:T(8,128)(2,1)}, u32[]{:S(2)}, u32[]{:S(2)}) collective-permute-start(bf16[4,32,2048]{2,1,0:T(8,128)(2,1)} %slice.61), channel_id=1, source_target_pairs={{0,12},{1,13},{2,14},{3,15},{4,0},{5,1},{6,2},{7,3},{8,4},{9,5},{1... | collective-permute-start | bytes 1572872 | tf_op jit(solution)/shard_map/ppermute | solution.py:260
  170.7 3.1 %shard_map.126.refs_3_ = f32[128,2048]{1,0:T(8,128)S(1)} custom-call(s32[1]{0:T(128)} %bitcast.me_ref, bf16[16,64,128]{2,1,0:T(8,128)(2,1)S(1)} %bitcast.30, bf16[8,32,2048]{2,1,0:T(8,128)(2,1)S(1)} %pad_maximum_fusion.refs_1_, bf16[8,32,2048]{2,1,0:T(8,128)(2,1)} %collective-permute-done.8.refs_2_, bf16[8,32,2048]{2,1,0:T(8,128)(2,1)S(1)} %collective-permute-done.6.refs_3_), custom_call_target="tpu_custom_call" | custom-call | flops 402653184 | bytes 4456448 | tf_op jit(solution)/shard_map/pallas_call | solution.py:146
  173.8 3.1 %collective-permute-done.9.refs_2_ = bf16[4,32,2048]{2,1,0:T(8,128)(2,1)} collective-permute-done((bf16[4,32,2048]{2,1,0:T(8,128)(2,1)}, bf16[4,32,2048]{2,1,0:T(8,128)(2,1)}, u32[]{:S(2)}, u32[]{:S(2)}) %collective-permute-start.9) | collective-permute-done | bytes 524320 | tf_op jit(solution)/shard_map/ppermute | solution.py:260
  176.9 3.8 %shard_map.127 = bf16[2048,128]{1,0:T(8,128)(2,1)} custom-call(s32[1]{0:T(128)} %bitcast.me_ref, bf16[16,64,128]{2,1,0:T(8,128)(2,1)S(1)} %bitcast.31, bf16[4,32,2048]{2,1,0:T(8,128)(2,1)S(1)} %collective-permute-done.7.refs_1_, bf16[4,32,2048]{2,1,0:T(8,128)(2,1)} %collective-permute-done.9.refs_2_, f32[128,2048]{1,0:T(8,128)S(1)} %shard_map.126.refs_3_), custom_call_target="tpu_custom_call" | custom-call | flops 134217728 | bytes 2359296 | tf_op jit(solution)/shard_map/pallas_call | solution.py:146
  (47 shorter events, 17.1 us)
Async XLA Ops:
  0.6 24.1 %copy-start = (f32[3,1024]{1,0:T(4,128)S(1)}, f32[3,1024]{1,0:T(4,128)}, u32[]{:S(2)}) copy-start(f32[3,1024]{1,0:T(4,128)} %param.14) | copy-start | bytes 36868
  0.7 0.8 copy-start.2
  1.5 0.7 copy-start.3
  2.2 45.2 %copy-start.7 = (bf16[64,2048]{1,0:T(8,128)(2,1)S(1)}, bf16[64,2048]{1,0:T(8,128)(2,1)}, u32[]{:S(2)}) copy-start(bf16[64,2048]{1,0:T(8,128)(2,1)} %param.12) | copy-start | bytes 786436
  3.4 29.5 %all-to-all-start = ((bf16[16,2,32,128]{3,2,1,0:T(8,128)(2,1)}), bf16[16,2,32,128]{3,2,1,0:T(8,128)(2,1)S(1)}, u32[]{:S(2)}, u32[]{:S(2)}) async-start(bf16[16,2,32,128]{3,2,1,0:T(8,128)(2,1)} %bitcast.2), calls=%async_computation | async-start | bytes 524288 | tf_op jit(solution)/shard_map/all_to_all | solution.py:226
  20.3 20.8 %collective-permute-start.1 = (bf16[64,2]{1,0:T(8,128)(2,1)S(1)}, bf16[64,2]{1,0:T(8,128)(2,1)S(1)}, u32[]{:S(2)}, u32[]{:S(2)}) collective-permute-start(bf16[64,2]{1,0:T(8,128)(2,1)S(1)} %slice.54), channel_id=1, source_target_pairs={{0,16},{16,32},{32,48},{48,64},{64,80},{80,96},{96,112},{112,128},... | collective-permute-start | bytes 776 | tf_op jit(solution)/shard_map/ppermute | solution.py:234
  32.9 9.1 %collective-permute-start = (bf16[512,128]{1,0:T(8,128)(2,1)S(1)}, bf16[512,128]{1,0:T(8,128)(2,1)S(1)}, u32[]{:S(2)}, u32[]{:S(2)}) collective-permute-start(bf16[512,128]{1,0:T(8,128)(2,1)S(1)} %bitcast.43), channel_id=1, source_target_pairs={{0,16},{16,0},{1,17},{17,1},{2,18},{18,2},{3,19},{19,3},{4,20},{20... | collective-permute-start | bytes 393224 | tf_op jit(solution)/shard_map/ppermute | solution.py:274
  43.2 21.0 %all-to-all-start.1 = ((bf16[4,1024,128]{2,1,0:T(8,128)(2,1)}), bf16[4,1024,128]{2,1,0:T(8,128)(2,1)S(1)}, u32[]{:S(2)}, u32[]{:S(2)}) async-start(bf16[4,1024,128]{2,1,0:T(8,128)(2,1)} %broadcast_in_dim.4), calls=%async_computation.1 | async-start | bytes 2097152 | tf_op jit(solution)/shard_map/all_to_all | solution.py:269
  47.7 11.0 %collective-permute-start.2 = (bf16[2,32,2048]{2,1,0:T(8,128)(2,1)S(1)}, bf16[2,32,2048]{2,1,0:T(8,128)(2,1)S(1)}, u32[]{:S(2)}, u32[]{:S(2)}) collective-permute-start(bf16[2,32,2048]{2,1,0:T(8,128)(2,1)S(1)} %bitcast.37), channel_id=1, source_target_pairs={{0,3},{1,0},{2,1},{3,2},{4,7},{5,4},{6,5},{7,6},{8,11},{9,8},{10,9... | collective-permute-start | bytes 786440 | tf_op jit(solution)/shard_map/ppermute | solution.py:260
  52.3 8.9 %collective-permute-start.3 = (bf16[2,32,2048]{2,1,0:T(8,128)(2,1)S(1)}, bf16[2,32,2048]{2,1,0:T(8,128)(2,1)S(1)}, u32[]{:S(2)}, u32[]{:S(2)}) collective-permute-start(bf16[2,32,2048]{2,1,0:T(8,128)(2,1)S(1)} %bitcast.38), channel_id=1, source_target_pairs={{0,2},{1,3},{2,0},{3,1},{4,6},{5,7},{6,4},{7,5},{8,10},{9,11},{10,... | collective-permute-start | bytes 786440 | tf_op jit(solution)/shard_map/ppermute | solution.py:260
  54.8 9.2 %collective-permute-start.4 = (bf16[2,32,2048]{2,1,0:T(8,128)(2,1)S(1)}, bf16[2,32,2048]{2,1,0:T(8,128)(2,1)S(1)}, u32[]{:S(2)}, u32[]{:S(2)}) collective-permute-start(bf16[2,32,2048]{2,1,0:T(8,128)(2,1)S(1)} %bitcast.39), channel_id=1, source_target_pairs={{0,1},{1,2},{2,3},{3,0},{4,5},{5,6},{6,7},{7,4},{8,9},{9,10},{10,1... | collective-permute-start | bytes 786440 | tf_op jit(solution)/shard_map/ppermute | solution.py:260
  65.0 30.7 %copy-start.4 = (bf16[1,2048,256]{2,1,0:T(8,128)(2,1)S(1)}, bf16[1,2048,256]{2,1,0:T(8,128)(2,1)}, u32[]{:S(2)}) copy-start(bf16[1,2048,256]{2,1,0:T(8,128)(2,1)} %param.19) | copy-start | bytes 3145732
  65.0 30.7 %copy-start.5 = (bf16[1,2048,256]{2,1,0:T(8,128)(2,1)S(1)}, bf16[1,2048,256]{2,1,0:T(8,128)(2,1)}, u32[]{:S(2)}) copy-start(bf16[1,2048,256]{2,1,0:T(8,128)(2,1)} %param.20) | copy-start | bytes 3145732
  65.0 30.7 %copy-start.6 = (bf16[1,256,2048]{2,1,0:T(8,128)(2,1)S(1)}, bf16[1,256,2048]{2,1,0:T(8,128)(2,1)}, u32[]{:S(2)}) copy-start(bf16[1,256,2048]{2,1,0:T(8,128)(2,1)} %param.21) | copy-start | bytes 3145732
  133.1 37.4 %copy-start.8 = (f32[256,2]{0,1:T(2,128)S(1)}, f32[256,2]{0,1:T(2,128)}, u32[]{:S(2)}) copy-start(f32[256,2]{0,1:T(2,128)} %param.18) | copy-start | bytes 6148
  133.1 37.6 %copy-start.1 = (bf16[1024,128]{1,0:T(8,128)(2,1)S(1)}, bf16[1024,128]{1,0:T(8,128)(2,1)}, u32[]{:S(2)}) copy-start(bf16[1024,128]{1,0:T(8,128)(2,1)} %param.15) | copy-start | bytes 786436
  133.1 13.5 %all-to-all-start.4 = ((bf16[4,1024,128]{2,1,0:T(8,128)(2,1)}), bf16[4,1024,128]{2,1,0:T(8,128)(2,1)S(1)}, u32[]{:S(2)}, u32[]{:S(2)}) async-start(bf16[4,1024,128]{2,1,0:T(8,128)(2,1)} %bitcast.15), calls=%async_computation.4 | async-start | bytes 2097152 | tf_op jit(solution)/shard_map/all_to_all | solution.py:269
  136.8 24.5 %collective-permute-start.6 = (bf16[8,32,2048]{2,1,0:T(8,128)(2,1)S(1)}, bf16[8,32,2048]{2,1,0:T(8,128)(2,1)S(1)}, u32[]{:S(2)}, u32[]{:S(2)}) collective-permute-start(bf16[8,32,2048]{2,1,0:T(8,128)(2,1)S(1)} %pad_maximum_fusion.refs_1_), channel_id=1, source_target_pairs={{0,4},{1,5},{2,6},{3,7},{4,8},{5,9},{6,10},{7,11},{8,12},{9,13},{1... | collective-permute-start | bytes 3145736 | tf_op jit(solution)/shard_map/ppermute | solution.py:260
  140.1 24.2 %collective-permute-start.8 = (bf16[8,32,2048]{2,1,0:T(8,128)(2,1)S(1)}, bf16[8,32,2048]{2,1,0:T(8,128)(2,1)}, u32[]{:S(2)}, u32[]{:S(2)}) collective-permute-start(bf16[8,32,2048]{2,1,0:T(8,128)(2,1)S(1)} %pad_maximum_fusion.refs_1_), channel_id=1, source_target_pairs={{0,12},{1,13},{2,14},{3,15},{4,0},{5,1},{6,2},{7,3},{8,4},{9,5},{1... | collective-permute-start | bytes 3145736 | tf_op jit(solution)/shard_map/ppermute | solution.py:260
  146.9 8.6 %collective-permute-start.5 = (bf16[512,128]{1,0:T(8,128)(2,1)S(1)}, bf16[512,128]{1,0:T(8,128)(2,1)S(1)}, u32[]{:S(2)}, u32[]{:S(2)}) collective-permute-start(bf16[512,128]{1,0:T(8,128)(2,1)S(1)} %get-tuple-element.25), channel_id=1, source_target_pairs={{0,16},{16,0},{1,17},{17,1},{2,18},{18,2},{3,19},{19,3},{4,20},{20... | collective-permute-start | bytes 393224 | tf_op jit(solution)/shard_map/ppermute | solution.py:291
  156.2 24.5 %all-to-all-start.5 = ((bf16[16,2,32,128]{3,2,1,0:T(8,128)(2,1)}), bf16[16,2,32,128]{3,2,1,0:T(8,128)(2,1)S(1)}, u32[]{:S(2)}, u32[]{:S(2)}) async-start(bf16[16,2,32,128]{3,2,1,0:T(8,128)(2,1)} %pad_maximum_fusion.2), calls=%async_computation.5 | async-start | bytes 524288 | tf_op jit(solution)/shard_map/all_to_all | solution.py:301
  162.1 11.7 %collective-permute-start.7 = (bf16[4,32,2048]{2,1,0:T(8,128)(2,1)}, bf16[4,32,2048]{2,1,0:T(8,128)(2,1)S(1)}, u32[]{:S(2)}, u32[]{:S(2)}) collective-permute-start(bf16[4,32,2048]{2,1,0:T(8,128)(2,1)} %slice.60), channel_id=1, source_target_pairs={{0,4},{1,5},{2,6},{3,7},{4,8},{5,9},{6,10},{7,11},{8,12},{9,13},{1... | collective-permute-start | bytes 1572872 | tf_op jit(solution)/shard_map/ppermute | solution.py:260
  166.2 10.7 %collective-permute-start.9 = (bf16[4,32,2048]{2,1,0:T(8,128)(2,1)}, bf16[4,32,2048]{2,1,0:T(8,128)(2,1)}, u32[]{:S(2)}, u32[]{:S(2)}) collective-permute-start(bf16[4,32,2048]{2,1,0:T(8,128)(2,1)} %slice.61), channel_id=1, source_target_pairs={{0,12},{1,13},{2,14},{3,15},{4,0},{5,1},{6,2},{7,3},{8,4},{9,5},{1... | collective-permute-start | bytes 1572872 | tf_op jit(solution)/shard_map/ppermute | solution.py:260
